TPU v7x, 256 devices: a whole 4x4x8 slice. The times are simulated.
256 devices in a mesh: sp: 64 (over z, x, core), tp: 4 (over y).
Axes of the slice: x: 4, y: 4, z: 8, core: 2. Of those that a mesh axis runs over, the one named last changes fastest.
Arguments:
- layer_input: bfloat16 [10240, 4096], P('sp', 'tp'), may hold values from -24 to 24
- output_grad: bfloat16 [10240, 4096], P('sp', 'tp'), may hold values from -64 to 64
- query_weight: bfloat16 [4096, 2048], P(None, 'tp'), may hold values from -0.09375 to 0.09375
- key_weight: bfloat16 [4096, 1024], P(None, 'tp'), may hold values from -0.09375 to 0.09375
- value_weight: bfloat16 [4096, 1024], P(None, 'tp'), may hold values from -0.09375 to 0.09375
- out_weight: bfloat16 [2048, 4096], P('tp'), may hold values from -0.125 to 0.125
- sink_logit: float32 [16], P('tp'), may hold values from 3 to 7
Outputs:
- input_grad: bfloat16 [10240, 4096], P('sp', 'tp')
- query_weight_grad: float32 [4096, 2048], P('sp', 'tp')
- key_weight_grad: float32 [4096, 1024], P('sp', 'tp')
- value_weight_grad: float32 [4096, 1024], P('sp', 'tp')
- out_weight_grad: float32 [2048, 4096], P('tp', 'sp')
- sink_grad: float32 [16], P('tp')
All inputs are finite; a program needn't handle non-finite values.
Results may differ from a plain program's by a relative error of at most 0.015.
Values may be sent and summed in bfloat16 or wider, within the bound.
A program may use at most 192 MiB of HBM per device.

v0:
```python
import jax
import jax.numpy as jnp
from jax import lax
from jax.sharding import PartitionSpec as P

HEADS = 16
KV_HEADS = 8
HEAD = 128
WINDOW = 128


masked_score = -1e30


def sent_together(arrays, axis, dim, along):
    widths = [a.shape[along] for a in arrays]
    both = jnp.concatenate(arrays, axis=along)
    result = lax.all_gather(both, axis, axis=dim, tiled=True)
    return tuple(jnp.split(result, [sum(widths[:k]) for k in range(1, len(widths))], axis=along))


def extended(cells, sides, width):
    for axis, dim in sides:
        count = lax.axis_size(axis)
        ends = count - 1
        head = lax.slice_in_dim(cells, 0, width, axis=dim)
        tail = lax.slice_in_dim(cells, cells.shape[dim] - width, cells.shape[dim], axis=dim)
        cells = jnp.concatenate(
            [
                lax.ppermute(tail, axis, [(i, (i + 1) % count) for i in range(ends)]),
                cells,
                lax.ppermute(head, axis, [((i + 1) % count, i) for i in range(ends)]),
            ],
            axis=dim,
        )
    return cells


def sent_to_all(array, axis):
    copies = jnp.broadcast_to(array, (lax.axis_size(axis), *array.shape))
    return lax.all_to_all(copies, axis, split_axis=0, concat_axis=0, tiled=True)


def taken_together(array, axis):
    everything = sent_to_all(array, axis)
    return jnp.sum(everything, axis=0)


def passed_along(value, axis, steps):
    count = lax.axis_size(axis)
    initial, last = (max(0, -steps), min(count, count - steps))
    return lax.ppermute(value, axis, [(source, source + steps) for source in range(initial, last)])


def split_up(array, dim, devices):
    shape = array.shape
    tiles = array.reshape(*shape[:dim], devices, shape[dim] // devices, *shape[dim + 1 :])
    return jnp.moveaxis(tiles, dim, 0)


def sum_at_owner(array, axis, dim):
    devices = lax.axis_size(axis)
    tiles = lax.all_to_all(split_up(array, dim, devices), axis, 0, 0, tiled=True)
    return jnp.sum(tiles.astype(jnp.float32), axis=0)


def contract_rows(left, right):
    return lax.dot_general(
        left, right, (((0,), (0,)), ((), ())), preferred_element_type=jnp.float32
    )


def contract_cols(left, right):
    return lax.dot_general(
        left, right, (((1,), (1,)), ((), ())), preferred_element_type=jnp.float32
    )


def per_device(
    layer_input, output_grad, query_weight, key_weight, value_weight, out_weight, sink_logit
):
    whole_input, whole_grad = sent_together((layer_input, output_grad), "tp", 1, 0)
    tok_rows = whole_input.shape[0]
    query_cols = query_weight.shape[1]
    key_cols = key_weight.shape[1]
    key_heads = key_cols // HEAD
    group_size = HEADS // KV_HEADS
    scaling = HEAD ** (-0.5)
    queries = jnp.dot(whole_input, query_weight, preferred_element_type=jnp.float32).astype(
        jnp.bfloat16
    )
    key_rows = jnp.dot(whole_input, key_weight, preferred_element_type=jnp.float32).astype(
        jnp.bfloat16
    )
    value_rows = jnp.dot(whole_input, value_weight, preferred_element_type=jnp.float32).astype(
        jnp.bfloat16
    )
    out_rows_grad = contract_cols(whole_grad, out_weight).astype(jnp.bfloat16)
    joined = jnp.concatenate([key_rows, value_rows], axis=1)
    band = extended(joined, (("sp", 0),), WINDOW)
    band_rows = band.shape[0]
    band_keys = band[:, :key_cols].reshape(band_rows, key_heads, HEAD)
    band_values = band[:, key_cols:].reshape(band_rows, key_heads, HEAD)
    shard_index = lax.axis_index("sp")
    seq_total = tok_rows * lax.axis_size("sp")
    query_pos = shard_index * tok_rows + jnp.arange(tok_rows, dtype=jnp.int32)
    key_pos = shard_index * tok_rows - WINDOW + jnp.arange(band_rows, dtype=jnp.int32)
    in_window = (
        (jnp.abs(query_pos[:, None] - key_pos[None, :]) <= WINDOW)
        & (key_pos[None, :] >= 0)
        & (key_pos[None, :] < seq_total)
    )
    query_heads = queries.reshape(tok_rows, key_heads, group_size, HEAD)
    grad_heads = out_rows_grad.reshape(tok_rows, key_heads, group_size, HEAD)
    scores = (
        jnp.einsum("qkgd,skd->kgqs", query_heads, band_keys, preferred_element_type=jnp.float32)
        * scaling
    )
    scores = jnp.where(in_window[None, None], scores, masked_score)
    sink_column = sink_logit.reshape(key_heads, group_size)[:, :, None]
    row_max = jnp.maximum(jnp.max(scores, axis=-1), sink_column)
    row_total = jnp.sum(jnp.exp(scores - row_max[..., None]), axis=-1) + jnp.exp(
        sink_column - row_max
    )
    log_total = row_max + jnp.log(row_total)
    soft_weights = jnp.exp(scores - log_total[..., None])
    soft_rounded = soft_weights.astype(jnp.bfloat16)
    attended = jnp.einsum(
        "kgqs,skd->qkgd", soft_rounded, band_values, preferred_element_type=jnp.float32
    ).astype(jnp.bfloat16)
    row_dots = jnp.sum(
        grad_heads.astype(jnp.float32) * attended.astype(jnp.float32), axis=-1
    ).transpose(1, 2, 0)
    prob_grads = jnp.einsum(
        "qkgd,skd->kgqs", grad_heads, band_values, preferred_element_type=jnp.float32
    )
    score_grads = (soft_weights * (prob_grads - row_dots[..., None])).astype(jnp.bfloat16)
    query_grads = (
        jnp.einsum("kgqs,skd->qkgd", score_grads, band_keys, preferred_element_type=jnp.float32)
        * scaling
    )
    query_grads = query_grads.astype(jnp.bfloat16).reshape(tok_rows, query_cols)
    band_key_grads = (
        jnp.einsum("kgqs,qkgd->skd", score_grads, query_heads, preferred_element_type=jnp.float32)
        * scaling
    )
    band_value_grads = jnp.einsum(
        "kgqs,qkgd->skd", soft_rounded, grad_heads, preferred_element_type=jnp.float32
    )
    band_grads = jnp.concatenate(
        [
            band_key_grads.reshape(band_rows, key_cols),
            band_value_grads.reshape(band_rows, key_cols),
        ],
        axis=1,
    )
    sink_part = -jnp.sum(jnp.exp(sink_column - log_total) * row_dots, axis=-1).reshape(-1)
    sink_grad = taken_together(sink_part, "sp")
    attended_rows = attended.reshape(tok_rows, query_cols)
    returned_low = passed_along(band_grads[:WINDOW].astype(jnp.bfloat16), "sp", -1).astype(
        jnp.float32
    )
    returned_high = passed_along(
        band_grads[band_rows - WINDOW :].astype(jnp.bfloat16), "sp", 1
    ).astype(jnp.float32)
    own_rows = band_grads[WINDOW : WINDOW + tok_rows]
    own_rows = own_rows.at[tok_rows - WINDOW :].add(returned_low)
    own_rows = own_rows.at[:WINDOW].add(returned_high)
    key_grads = own_rows[:, :key_cols].astype(jnp.bfloat16)
    value_grads = own_rows[:, key_cols:].astype(jnp.bfloat16)
    all_sums = lax.psum_scatter(
        jnp.concatenate(
            [
                contract_rows(whole_input, query_grads),
                contract_rows(whole_grad, attended_rows),
                contract_rows(whole_input, key_grads),
                contract_rows(whole_input, value_grads),
            ],
            axis=1,
        ),
        "sp",
        scatter_dimension=0,
        tiled=True,
    )
    query_part = all_sums[:, :query_cols]
    out_part = all_sums[:, query_cols : 2 * query_cols]
    key_part = all_sums[:, 2 * query_cols : 2 * query_cols + key_cols]
    value_part = all_sums[:, 2 * query_cols + key_cols :]
    partials = (
        contract_cols(query_grads, query_weight)
        + contract_cols(key_grads, key_weight)
        + contract_cols(value_grads, value_weight)
    )
    input_grad = sum_at_owner(partials.astype(jnp.bfloat16), "tp", 1).astype(jnp.bfloat16)
    return (input_grad, query_part, key_part, value_part, out_part.T, sink_grad)


def solution(mesh):
    placed = (
        P("sp", "tp"),
        P("sp", "tp"),
        P(None, "tp"),
        P(None, "tp"),
        P(None, "tp"),
        P("tp", None),
        P("tp"),
    )
    return jax.shard_map(
        per_device,
        mesh=mesh,
        in_specs=placed,
        out_specs=(
            P("sp", "tp"),
            P("sp", "tp"),
            P("sp", "tp"),
            P("sp", "tp"),
            P("tp", "sp"),
            P("tp"),
        ),
        check_vma=False,
    )
```

profile of v0, /device:TPU:2, one launch (start us, length us, event | category | flops | bytes accessed | tf_op | source)
XLA Modules:
  0.0 362.0 jit_solution(8738537586220035245)
XLA Ops:
  7.2 2.1 pad_maximum_fusion.1
  10.4 40.1 %all-gather.2.cloned.1.call-done = bf16[320,4096]{1,0:T(8,128)(2,1)} async-done(((bf16[320,1024]{1,0:T(8,128)(2,1)}), bf16[320,4096]{1,0:T(8,128)(2,1)}) %all-gather.2.cloned.1.call-update) | async-done | bytes 2621456 | tf_op jit(solution)/shard_map/all_gather | solution.py:18
  50.5 2.0 convolution_convert_fusion.3
  52.6 2.3 convolution_convert_fusion.4
  54.9 1.9 collective-permute-start
  56.9 3.9 %collective-permute-start.1 = (bf16[128,512]{1,0:T(8,128)(2,1)S(1)}, bf16[128,512]{1,0:T(8,128)(2,1)S(1)}, u32[]{:S(2)}, u32[]{:S(2)}) collective-permute-start(bf16[128,512]{1,0:T(8,128)(2,1)S(1)} %get-tuple-element.69), channel_id=1, source_target_pairs={{4,0},{8,4},{12,8},{16,12},{20,16},{24,20},{28,24},{32,28},{36,32}... | collective-permute-start | bytes 393224 | tf_op jit(solution)/shard_map/ppermute | solution.py:32
  61.7 1.5 convolution_convert_fusion.1
  67.7 3.7 %collective-permute-start.3 = (bf16[128,512]{1,0:T(8,128)(2,1)S(1)}, bf16[128,512]{1,0:T(8,128)(2,1)S(1)}, u32[]{:S(2)}, u32[]{:S(2)}) collective-permute-start(bf16[128,512]{1,0:T(8,128)(2,1)S(1)} %get-tuple-element.60), channel_id=1, source_target_pairs={{0,4},{4,8},{8,12},{12,16},{16,20},{20,24},{24,28},{28,32},{32,36}... | collective-permute-start | bytes 393224 | tf_op jit(solution)/shard_map/ppermute | solution.py:52
  71.4 2.1 collective-permute-start.2
  73.5 4.5 %fusion.20 = f32[4096,512]{0,1:T(8,128)} fusion(bf16[160,512]{1,0:T(8,128)(2,1)S(1)} %reshape.187, bf16[320,4096]{1,0:T(8,128)(2,1)S(1)} %copy-done.2), kind=kOutput, calls=%fused_computation.36 | convolution fusion | flops 671088640 | bytes 9863168 | tf_op jit(solution)/shard_map/dot_general | solution.py:68
  78.0 4.5 %fusion.11 = f32[4096,512]{0,1:T(8,128)} fusion(bf16[160,512]{1,0:T(8,128)(2,1)S(1)} %reshape.191, bf16[320,4096]{1,0:T(8,128)(2,1)S(1)} %copy-done.2), kind=kOutput, calls=%fused_computation.24 | convolution fusion | flops 671088640 | bytes 9863168 | tf_op jit(solution)/shard_map/dot_general | solution.py:68
  83.5 2.7 fusion.16
  86.2 17.1 %pad_maximum_fusion = f32[4096,1536]{0,1:T(8,128)} fusion(f32[4096,256]{0,1:T(8,128)} %fusion.16, f32[4096,256]{0,1:T(8,128)S(1)} %fusion.18, f32[4096,512]{0,1:T(8,128)} %fusion.11, f32[4096,512]{0,1:T(8,128)} %fusion.20), kind=kLoop, calls=%fused_computation | loop fusion | flops 18874368 | bytes 50331648 | tf_op jit(solution)/shard_map/concatenate | solution.py:172
  103.3 24.7 %copy.112 = f32[4096,1536]{1,0:T(8,128)} copy(f32[4096,1536]{0,1:T(8,128)} %pad_maximum_fusion) | data formatting | bytes 50331648
  128.8 14.8 %all-to-all-start.1 = ((f32[64,1,4]{2,1,0:T(1,128)}), f32[64,1,4]{2,1,0:T(1,128)S(1)}, u32[]{:S(2)}, u32[]{:S(2)}) async-start(f32[64,1,4]{2,1,0:T(1,128)} %broadcast_in_dim.16), calls=%async_computation.1 | async-start | bytes 65536 | tf_op jit(solution)/shard_map/all_to_all | solution.py:41
  146.2 1.7 copy-done.4
  147.9 1.6 fusion.1
  149.4 1.2 copy.149
  150.6 1.5 all-to-all-done.1
  152.2 3.6 all-to-all-start
  156.3 17.6 %all-to-all-done = bf16[4,160,1024]{2,1,0:T(8,128)(2,1)S(1)} async-done(((bf16[4,160,1024]{2,1,0:T(8,128)(2,1)}), bf16[4,160,1024]{2,1,0:T(8,128)(2,1)S(1)}, u32[]{:S(2)}, u32[]{:S(2)}) %all-to-all-start) | async-done | bytes 1310752 | tf_op jit(solution)/shard_map/all_to_all | solution.py:63
  174.9 177.0 %reduce-scatter.4.cloned.1.call-done = f32[64,1536]{1,0:T(8,128)} async-done(((f32[4096,1536]{1,0:T(8,128)}), f32[64,1536]{1,0:T(8,128)}) %reduce-scatter.4.cloned.1.call-update) | async-done | bytes 393232
  351.9 1.5 fusion.50
  353.4 1.7 slice_bitcast_fusion
  (64 shorter events, 12.4 us)
Async XLA Ops:
  7.2 43.3 %copy-start = (bf16[4096,256]{1,0:T(8,128)(2,1)S(1)}, bf16[4096,256]{1,0:T(8,128)(2,1)}, u32[]{:S(2)}) copy-start(bf16[4096,256]{1,0:T(8,128)(2,1)} %param.15) | copy-start | bytes 6291460
  7.2 43.3 %all-gather.2.cloned.1.call-start = ((), (), s32[]{:S(2)}) async-start(), calls=%async_computation.3 | async-start | bytes 3276800 | tf_op jit(solution)/shard_map/all_gather | solution.py:18
  9.4 342.6 %reduce-scatter.4.cloned.1.call-start = ((), (), s32[]{:S(2)}) async-start(), calls=%async_computation.4 | async-start | bytes 25559040
  50.5 2.1 copy-start.1
  52.6 8.2 %copy-start.3 = (bf16[4096,512]{1,0:T(8,128)(2,1)S(1)}, bf16[4096,512]{1,0:T(8,128)(2,1)}, u32[]{:S(2)}) copy-start(bf16[4096,512]{1,0:T(8,128)(2,1)} %param.13) | copy-start | bytes 12582916
  54.9 8.4 %collective-permute-start = (bf16[128,512]{1,0:T(8,128)(2,1)S(1)}, bf16[128,512]{1,0:T(8,128)(2,1)S(1)}, u32[]{:S(2)}, u32[]{:S(2)}) collective-permute-start(bf16[128,512]{1,0:T(8,128)(2,1)S(1)} %get-tuple-element.68), channel_id=1, source_target_pairs={{0,4},{4,8},{8,12},{12,16},{16,20},{20,24},{24,28},{28,32},{32,36}... | collective-permute-start | bytes 393224 | tf_op jit(solution)/shard_map/ppermute | solution.py:30
  56.9 4.8 %copy-start.6 = (bf16[512,4096]{1,0:T(8,128)(2,1)S(1)}, bf16[512,4096]{1,0:T(8,128)(2,1)}, u32[]{:S(2)}) copy-start(bf16[512,4096]{1,0:T(8,128)(2,1)} %param.16) | copy-start | bytes 12582916
  56.9 6.4 %collective-permute-start.1 = (bf16[128,512]{1,0:T(8,128)(2,1)S(1)}, bf16[128,512]{1,0:T(8,128)(2,1)S(1)}, u32[]{:S(2)}, u32[]{:S(2)}) collective-permute-start(bf16[128,512]{1,0:T(8,128)(2,1)S(1)} %get-tuple-element.69), channel_id=1, source_target_pairs={{4,0},{8,4},{12,8},{16,12},{20,16},{24,20},{28,24},{32,28},{36,32}... | collective-permute-start | bytes 393224 | tf_op jit(solution)/shard_map/ppermute | solution.py:32
  67.5 6.0 %copy-start.2 = (bf16[320,4096]{1,0:T(8,128)(2,1)S(1)}, bf16[320,4096]{1,0:T(8,128)(2,1)}, u32[]{:S(2)}) copy-start(bf16[320,4096]{1,0:T(8,128)(2,1)} %all-gather.2.cloned.1.call-done) | copy-start | bytes 7864324
  67.7 14.9 %collective-permute-start.3 = (bf16[128,512]{1,0:T(8,128)(2,1)S(1)}, bf16[128,512]{1,0:T(8,128)(2,1)S(1)}, u32[]{:S(2)}, u32[]{:S(2)}) collective-permute-start(bf16[128,512]{1,0:T(8,128)(2,1)S(1)} %get-tuple-element.60), channel_id=1, source_target_pairs={{0,4},{4,8},{8,12},{12,16},{16,20},{20,24},{24,28},{28,32},{32,36}... | collective-permute-start | bytes 393224 | tf_op jit(solution)/shard_map/ppermute | solution.py:52
  71.4 11.2 %collective-permute-start.2 = (bf16[128,512]{1,0:T(8,128)(2,1)S(1)}, bf16[128,512]{1,0:T(8,128)(2,1)S(1)}, u32[]{:S(2)}, u32[]{:S(2)}) collective-permute-start(bf16[128,512]{1,0:T(8,128)(2,1)S(1)} %get-tuple-element.61), channel_id=1, source_target_pairs={{4,0},{8,4},{12,8},{16,12},{20,16},{24,20},{28,24},{32,28},{36,32}... | collective-permute-start | bytes 393224 | tf_op jit(solution)/shard_map/ppermute | solution.py:52
  128.8 23.3 %all-to-all-start.1 = ((f32[64,1,4]{2,1,0:T(1,128)}), f32[64,1,4]{2,1,0:T(1,128)S(1)}, u32[]{:S(2)}, u32[]{:S(2)}) async-start(f32[64,1,4]{2,1,0:T(1,128)} %broadcast_in_dim.16), calls=%async_computation.1 | async-start | bytes 65536 | tf_op jit(solution)/shard_map/all_to_all | solution.py:41
  143.6 1.7 copy-start.5
  145.4 2.5 copy-start.4
  152.2 21.7 %all-to-all-start = ((bf16[4,160,1024]{2,1,0:T(8,128)(2,1)}), bf16[4,160,1024]{2,1,0:T(8,128)(2,1)S(1)}, u32[]{:S(2)}, u32[]{:S(2)}) async-start(bf16[4,160,1024]{2,1,0:T(8,128)(2,1)} %bitcast.64), calls=%async_computation | async-start | bytes 2621440 | tf_op jit(solution)/shard_map/all_to_all | solution.py:63
Sparse Core Ops, SparseCore 0:
  9.8 40.6 all-gather.1
  128.1 223.7 reduce-scatter.3
where the time goes:
time: 364 us; the launch traced here: 362 us
  waiting for transfers between devices  236 us (65%)
  local copies, waits for them, and re-layouts  34 us (9%)
  starting transfers between devices  30 us (8%)
  matrix products  25.3 us (7%)
  other arithmetic  22 us (6%)
  between operations  14.4 us (4%)
    unnamed x3, waiting for transfers between devices  177 us
    all_gather x1, waiting for transfers between devices, sent_together(): result = lax.all_gather(both, axis, axis=dim, tiled=True)  40.1 us
    unnamed x16, local copies, waits for them, and re-layouts  27.4 us
    all_to_all x1, waiting for transfers between devices, sum_at_owner(): lax.all_to_all(split_up(array, dim, devices), axis, 0, 0, tiled=True)  17.6 us
    concatenate x1, other arithmetic, per_device(): jnp.concatenate([contract_rows(whole_input, query_grads), contract_rows(w...  17.1 us
    all_to_all x1, starting transfers between devices, sent_to_all(): return lax.all_to_all(copies, axis, split_axis=0, concat_axis=0, tiled=True)  14.8 us
    dot_general x4, matrix products, contract_rows(): lax.dot_general(left, right, (((0,), (0,)), ((), ())), preferred_element_...  12.5 us
  transfers between devices with their start and end apart: 8, of which 4 were waited for; matrix products, arithmetic and copies ran while one was open for 5% of the time, Pallas kernels for 0%

commit v1 on v0

v1 whole, which is shorter than its diff:
```python
import jax
import jax.numpy as jnp
from jax import lax
from jax.experimental import pallas as pl
from jax.experimental.pallas import tpu as pltpu
from jax.sharding import PartitionSpec as P

HEAD = 128
WINDOW = 128
NZ, NX, NC, NY = 8, 4, 2, 4
TOK = 160
SEQ = TOK * NZ * NX * NC
BAND = TOK + 2 * WINDOW
QC = 512
KC = 256
SCALING = HEAD ** (-0.5)
MASKED = -1e30
BF = jnp.bfloat16
F32 = jnp.float32
COPIES = 160


def mm(left, right, left_dim, right_dim):
    return lax.dot_general(
        left, right, (((left_dim,), (right_dim,)), ((), ())), preferred_element_type=F32
    )


def kernel(
    x_hbm, g_hbm, wq_hbm, wk_hbm, wv_hbm, wo_hbm, sink_ref,
    dx_out, wq_out, wk_out, wv_out, wo_out, sink_out,
    xg, dg, xc, dc, rx, rd, wq, wk, wv, wo, acc, dacc, band, queries, grads,
    soft, psink, gc, kvg, hs, hr, pf, pb, sr, zs, zr, ys, yr, yrelay, dxo, skx, skc, skz,
    local_sem, send_sem, recv_sem,
):
    sp = lax.axis_index("sp")
    y = lax.axis_index("tp")
    z = sp // (NX * NC)
    x = lax.rem(sp // NC, NX)
    c = lax.rem(sp, NC)

    def at_y(step):
        return (sp, lax.rem(y + step, NY))

    def at_x(step):
        return ((z * NX + lax.rem(x + step, NX)) * NC + c, y)

    def at_z(step):
        return ((lax.rem(z + step, NZ) * NX + x) * NC + c, y)

    sister = (sp + 1 - 2 * c, y)
    after = (lax.rem(sp + 1, NZ * NX * NC), y)
    before = (lax.rem(sp + NZ * NX * NC - 1, NZ * NX * NC), y)
    up, down = at_y(1), at_y(3)
    right, left = at_x(1), at_x(3)

    started = []
    local_count = [0]

    def send(src, dst, device):
        k = len(started)
        copy = pltpu.make_async_remote_copy(
            src_ref=src,
            dst_ref=dst,
            send_sem=send_sem.at[k],
            recv_sem=recv_sem.at[k],
            device_id=device,
            device_id_type=pl.DeviceIdType.MESH,
        )
        copy.start()
        started.append(copy)
        return copy

    def load(src, dst):
        k = local_count[0]
        local_count[0] += 1
        copy = pltpu.make_async_copy(src, dst, local_sem.at[k])
        copy.start()
        return copy

    def loads(hbm, blocks):
        return [
            [
                load(hbm.at[:, pl.ds((h * 4 + k) * 128, 128)], blocks.at[0, h, k])
                for k in range(4)
            ]
            for h in range(2)
        ]

    x_loads = loads(x_hbm, xg)
    weight_loads = [load(wq_hbm, wq), load(wk_hbm, wk), load(wv_hbm, wv)]
    d_loads = loads(g_hbm, dg)
    out_load = load(wo_hbm, wo)

    barrier = pltpu.get_barrier_semaphore()
    peers = [up, down, right, left, at_x(2), sister, after, before]
    peers += [at_z(step) for step in range(1, NZ)]
    for peer in peers:
        pl.semaphore_signal(
            barrier, inc=1, device_id=peer, device_id_type=pl.DeviceIdType.MESH
        )
    pl.semaphore_wait(barrier, len(peers))

    def gather_start(blocks):
        return (
            send(blocks.at[0, 0], blocks.at[1, 0], up),
            send(blocks.at[0, 1], blocks.at[3, 1], down),
            send(blocks.at[0, 1], blocks.at[1, 1], up),
            send(blocks.at[0, 0], blocks.at[3, 0], down),
        )

    def gather_pass(blocks, first):
        first[0].wait_recv()
        a = send(blocks.at[1, 0], blocks.at[2, 0], up)
        first[1].wait_recv()
        b = send(blocks.at[3, 1], blocks.at[2, 1], down)
        return a, b

    def exchange(blocks, cells, relay, ry):
        xr, xo, xl = lax.rem(x + 1, NX), lax.rem(x + 2, NX), lax.rem(x + 3, NX)
        near = (
            send(blocks.at[ry, :, xr], cells.at[ry, :, 1], right),
            send(blocks.at[ry, :, xl], cells.at[ry, :, 3], left),
        )
        far = (
            send(blocks.at[ry, 0, xo], relay.at[ry, 0], right),
            send(blocks.at[ry, 1, xo], relay.at[ry, 1], left),
        )
        for h in range(2):
            cells[ry, h, 0] = blocks[ry, h, x]
        return near, far

    def exchange_pass(cells, relay, ry, far):
        far[0].wait_recv()
        a = send(relay.at[ry, 0], cells.at[ry, 0, 2], right)
        far[1].wait_recv()
        b = send(relay.at[ry, 1], cells.at[ry, 1, 2], left)
        return a, b

    def wide(blocks, ry):
        return jnp.concatenate([blocks[ry, h, k] for h in range(2) for k in range(4)], axis=1)

    def features(ry):
        return pl.multiple_of(lax.rem(y + NY - ry, NY) * 1024, 1024)

    def project(ry):
        rows = pl.ds(features(ry), 1024)
        block = wide(xg, ry)
        for cols, weight in (
            (slice(0, QC), wq),
            (slice(QC, QC + KC), wk),
            (slice(QC + KC, QC + 2 * KC), wv),
        ):
            term = mm(block, weight[rows, :], 1, 0)
            acc[:, cols] = term if ry == 0 else acc[:, cols] + term

    def project_grad(ry):
        cols = pl.ds(features(ry), 1024)
        term = mm(wide(dg, ry), wo[:, cols], 1, 1)
        dacc[...] = term if ry == 0 else dacc[...] + term

    for half in x_loads:
        for copy in half:
            copy.wait()
    x_first = gather_start(xg)
    x_ex = {0: exchange(xg, xc, rx, 0)}
    for copy in weight_loads:
        copy.wait()
    project(0)
    x_second = gather_pass(xg, x_first)
    for half in d_loads:
        for copy in half:
            copy.wait()
    d_first = gather_start(dg)
    x_passed = [exchange_pass(xc, rx, 0, x_ex[0][1])]
    x_first[2].wait_recv()
    x_ex[1] = exchange(xg, xc, rx, 1)
    x_first[3].wait_recv()
    x_ex[3] = exchange(xg, xc, rx, 3)
    project(1)
    project(3)
    for copy in x_second:
        copy.wait_recv()
    x_ex[2] = exchange(xg, xc, rx, 2)
    project(2)

    band[WINDOW : WINDOW + TOK, :] = acc[:, QC : QC + 2 * KC].astype(BF)
    queries[...] = acc[:, :QC].astype(BF)
    halo_after = send(band.at[pl.ds(TOK, WINDOW)], band.at[pl.ds(0, WINDOW)], after)
    halo_before = send(
        band.at[pl.ds(WINDOW, WINDOW)], band.at[pl.ds(WINDOW + TOK, WINDOW)], before
    )
    d_second = gather_pass(dg, d_first)
    for ry in (1, 3):
        x_passed.append(exchange_pass(xc, rx, ry, x_ex[ry][1]))
    out_load.wait()
    d_ex = {0: exchange(dg, dc, rd, 0)}
    project_grad(0)
    halo_after.wait_recv()
    halo_before.wait_recv()

    row = lax.broadcasted_iota(jnp.int32, (2 * TOK, BAND), 0)
    row = jnp.where(row >= TOK, row - TOK, row)
    col = lax.broadcasted_iota(jnp.int32, (2 * TOK, BAND), 1) - WINDOW
    key_pos = sp * TOK + col
    in_window = (jnp.abs(row - col) <= WINDOW) & (key_pos >= 0) & (key_pos < SEQ)
    second_head = lax.broadcasted_iota(jnp.int32, (2 * TOK, 1), 0) >= TOK

    def heads(ref, kh):
        cols = kh * 2 * HEAD
        return jnp.concatenate(
            [ref[:, cols : cols + HEAD], ref[:, cols + HEAD : cols + 2 * HEAD]], axis=0
        )

    def put_heads(group, kh, value):
        cols = kh * 2 * HEAD
        gc[group, 0, :, cols : cols + HEAD] = value[:TOK].astype(BF)
        gc[group, 0, :, cols + HEAD : cols + 2 * HEAD] = value[TOK:].astype(BF)

    for kh in range(2):
        keys = band[:, kh * HEAD : (kh + 1) * HEAD]
        values = band[:, KC + kh * HEAD : KC + (kh + 1) * HEAD]
        scores = mm(heads(queries, kh), keys, 1, 1) * SCALING
        scores = jnp.where(in_window, scores, MASKED)
        sink = jnp.where(second_head, sink_ref[2 * kh + 1], sink_ref[2 * kh])
        row_max = jnp.maximum(jnp.max(scores, axis=1, keepdims=True), sink)
        weights = jnp.exp(scores - row_max)
        sink_weight = jnp.exp(sink - row_max)
        inverse = 1.0 / (jnp.sum(weights, axis=1, keepdims=True) + sink_weight)
        weights = weights * inverse
        soft[kh] = weights
        psink[kh] = sink_weight * inverse
        put_heads(0, kh, mm(weights.astype(BF), values, 1, 0))

    half = TOK // 2

    def share(group):
        own = gc.at[group, 0]
        low, high = pl.ds(0, half), pl.ds(half, half)
        return (
            send(own.at[low], gc.at[group, 1, low], right),
            send(own.at[high], gc.at[group, 3, high], left),
            send(own.at[high], gc.at[group, 1, high], right),
            send(own.at[low], gc.at[group, 3, low], left),
        )

    def share_pass(group, first):
        low, high = pl.ds(0, half), pl.ds(half, half)
        first[0].wait_recv()
        a = send(gc.at[group, 1, low], gc.at[group, 2, low], right)
        first[1].wait_recv()
        b = send(gc.at[group, 3, high], gc.at[group, 2, high], left)
        return a, b

    def arrived(first, second):
        for copy in first[2:] + second:
            copy.wait_recv()

    att_first = share(0)
    x_passed.append(exchange_pass(xc, rx, 2, x_ex[2][1]))
    d_passed = [exchange_pass(dc, rd, 0, d_ex[0][1])]
    d_first[2].wait_recv()
    d_ex[1] = exchange(dg, dc, rd, 1)
    d_first[3].wait_recv()
    d_ex[3] = exchange(dg, dc, rd, 3)
    project_grad(1)
    project_grad(3)
    att_second = share_pass(0, att_first)
    for copy in d_second:
        copy.wait_recv()
    d_ex[2] = exchange(dg, dc, rd, 2)
    project_grad(2)
    grads[...] = dacc[...].astype(BF)

    lane = lax.broadcasted_iota(jnp.int32, (8, 128), 1)
    sink_tile = jnp.zeros((8, 128), F32)
    for kh in range(2):
        keys = band[:, kh * HEAD : (kh + 1) * HEAD]
        values = band[:, KC + kh * HEAD : KC + (kh + 1) * HEAD]
        query = heads(queries, kh)
        grad = heads(grads, kh)
        attended = heads(gc.at[0, 0], kh)
        row_dots = jnp.sum(grad.astype(F32) * attended.astype(F32), axis=1, keepdims=True)
        weights = soft[kh]
        prob_grads = mm(grad, values, 1, 1)
        score_grads = (weights * (prob_grads - row_dots)).astype(BF)
        put_heads(1, kh, mm(score_grads, keys, 1, 0) * SCALING)
        kvg[:, kh * HEAD : (kh + 1) * HEAD] = mm(score_grads, query, 0, 0) * SCALING
        kvg[:, KC + kh * HEAD : KC + (kh + 1) * HEAD] = mm(weights.astype(BF), grad, 0, 0)
        sink_rows = psink[kh] * row_dots
        for g in range(2):
            total = -jnp.sum(sink_rows[g * TOK : (g + 1) * TOK], axis=0, keepdims=True)
            sink_tile = jnp.where(lane == 2 * kh + g, total, sink_tile)
    hs[0] = kvg[0:WINDOW, :].astype(BF)
    hs[1] = kvg[WINDOW + TOK : BAND, :].astype(BF)
    back = send(hs.at[0], hr.at[0], before)
    forth = send(hs.at[1], hr.at[1], after)
    q_first = share(1)
    skx[x] = sink_tile
    sink_x = [send(skx.at[x], skx.at[x], at_x(step)) for step in (1, 3, 2)]

    for ry in (1, 3):
        d_passed.append(exchange_pass(dc, rd, ry, d_ex[ry][1]))
    back.wait_recv()
    forth.wait_recv()
    kvg[WINDOW + TOK - WINDOW : WINDOW + TOK, :] += hr[0].astype(F32)
    kvg[WINDOW : 2 * WINDOW, :] += hr[1].astype(F32)
    gc[2, 0] = kvg[WINDOW : WINDOW + TOK, :].astype(BF)
    k_first = share(2)
    d_passed.append(exchange_pass(dc, rd, 2, d_ex[2][1]))
    q_second = share_pass(1, q_first)

    def input_share(step):
        rows = pl.ds(pl.multiple_of(lax.rem(y + step, NY) * 1024, 1024), 1024)
        return (
            mm(gc[1, 0], wq[rows, :], 1, 1)
            + mm(gc[2, 0, :, :KC], wk[rows, :], 1, 1)
            + mm(gc[2, 0, :, KC:], wv[rows, :], 1, 1)
        )

    ys[1] = input_share(2).astype(BF)
    y_far = (
        send(ys.at[1, pl.ds(0, half)], yrelay.at[0], up),
        send(ys.at[1, pl.ds(half, half)], yrelay.at[1], down),
    )
    ys[0] = input_share(1).astype(BF)
    y_near = [send(ys.at[0], yr.at[0], up)]
    ys[2] = input_share(3).astype(BF)
    y_near.append(send(ys.at[2], yr.at[2], down))
    k_second = share_pass(2, k_first)
    dxo[...] = input_share(0)

    for near, _ in list(x_ex.values()) + list(d_ex.values()):
        for copy in near:
            copy.wait_recv()
    for pair in x_passed + d_passed:
        for copy in pair:
            copy.wait_recv()
    for copy in sink_x:
        copy.wait_recv()
    skc[c] = (skx[0] + skx[1]) + (skx[2] + skx[3])
    sink_c = send(skc.at[c], skc.at[c], sister)

    def multiply(group, cells):
        rows = jnp.concatenate(
            [cells[ry, h].reshape(NX * TOK, 128) for ry in range(NY) for h in range(2)], axis=1
        )
        product = mm(rows, gc[group].reshape(NX * TOK, QC), 0, 0)
        product = product.reshape(NY, 2, NC, 64, QC)
        pf[group] = product
        pb[group] = product.astype(BF)
        return send(pb.at[group, :, :, 1 - c], sr.at[group], sister)

    def spread(group, from_sister):
        from_sister.wait_recv()
        for ry in range(NY):
            for h in range(2):
                zs[group, ry, h] = (pf[group, ry, h, c] + sr[group, ry, h].astype(F32)).astype(BF)
        copies = []
        for step in (4, 3, 5, 2, 6, 1, 7):
            to = lax.rem(z + step, NZ)
            ry = lax.rem(y + NY - to // 2, NY)
            copies.append(send(zs.at[group, ry, lax.rem(to, 2)], zr.at[group, step - 1], at_z(step)))
        return copies

    def collect(group, copies):
        ry = lax.rem(y + NY - z // 2, NY)
        h = lax.rem(z, 2)
        total = pf[group, ry, h, c] + sr[group, ry, h].astype(F32)
        for copy in copies:
            copy.wait_recv()
        for step in range(1, NZ):
            total = total + zr[group, step - 1].astype(F32)
        return total

    arrived(att_first, att_second)
    s0 = multiply(0, dc)
    y_far[0].wait_recv()
    y_pass = [send(yrelay.at[0], yr.at[1, pl.ds(0, half)], up)]
    y_far[1].wait_recv()
    y_pass.append(send(yrelay.at[1], yr.at[1, pl.ds(half, half)], down))
    arrived(q_first, q_second)
    s1 = multiply(1, xc)
    z0 = spread(0, s0)
    sink_c.wait_recv()
    skz[z] = skc[0] + skc[1]
    sink_z = [send(skz.at[z], skz.at[z], at_z(step)) for step in range(1, NZ)]
    arrived(k_first, k_second)
    s2 = multiply(2, xc)
    z1 = spread(1, s1)
    z2 = spread(2, s2)
    for copy in y_near + y_pass:
        copy.wait_recv()
    total = dxo[...]
    for k in range(3):
        total = total + yr[k].astype(F32)
    dx_out[...] = total.astype(BF)
    wo_out[...] = collect(0, z0).T
    wq_out[...] = collect(1, z1)
    for copy in sink_z:
        copy.wait_recv()
    total = skz[0]
    for k in range(1, NZ):
        total = total + skz[k]
    sink_out[...] = total
    last = collect(2, z2)
    wk_out[...] = last[:, :KC]
    wv_out[...] = last[:, KC:]
    for copy in started:
        copy.wait_send()


def per_device(
    layer_input, output_grad, query_weight, key_weight, value_weight, out_weight, sink_logit
):
    vmem = pltpu.VMEM
    anywhere = pl.BlockSpec(memory_space=pl.ANY)
    inside = pl.BlockSpec(memory_space=pltpu.VMEM)
    outs = pl.pallas_call(
        kernel,
        name="attention_backward",
        out_shape=(
            jax.ShapeDtypeStruct((TOK, 1024), BF),
            jax.ShapeDtypeStruct((64, QC), F32),
            jax.ShapeDtypeStruct((64, KC), F32),
            jax.ShapeDtypeStruct((64, KC), F32),
            jax.ShapeDtypeStruct((QC, 64), F32),
            jax.ShapeDtypeStruct((8, 128), F32),
        ),
        in_specs=[anywhere] * 6 + [pl.BlockSpec(memory_space=pltpu.SMEM)],
        out_specs=[inside] * 6,
        scratch_shapes=[
            vmem((NY, 2, 4, TOK, 128), BF),
            vmem((NY, 2, 4, TOK, 128), BF),
            vmem((NY, 2, NX, TOK, 128), BF),
            vmem((NY, 2, NX, TOK, 128), BF),
            vmem((NY, 2, TOK, 128), BF),
            vmem((NY, 2, TOK, 128), BF),
            vmem((4096, QC), BF),
            vmem((4096, KC), BF),
            vmem((4096, KC), BF),
            vmem((QC, 4096), BF),
            vmem((TOK, QC + 2 * KC), F32),
            vmem((TOK, QC), F32),
            vmem((BAND, 2 * KC), BF),
            vmem((TOK, QC), BF),
            vmem((TOK, QC), BF),
            vmem((2, 2 * TOK, BAND), F32),
            vmem((2, 2 * TOK, 1), F32),
            vmem((3, NX, TOK, QC), BF),
            vmem((BAND, 2 * KC), F32),
            vmem((2, WINDOW, 2 * KC), BF),
            vmem((2, WINDOW, 2 * KC), BF),
            vmem((3, NY, 2, NC, 64, QC), F32),
            vmem((3, NY, 2, NC, 64, QC), BF),
            vmem((3, NY, 2, 64, QC), BF),
            vmem((3, NY, 2, 64, QC), BF),
            vmem((3, NZ - 1, 64, QC), BF),
            vmem((3, TOK, 1024), BF),
            vmem((3, TOK, 1024), BF),
            vmem((2, TOK // 2, 1024), BF),
            vmem((TOK, 1024), F32),
            vmem((NX, 8, 128), F32),
            vmem((NC, 8, 128), F32),
            vmem((NZ, 8, 128), F32),
            pltpu.SemaphoreType.DMA((20,)),
            pltpu.SemaphoreType.DMA((COPIES,)),
            pltpu.SemaphoreType.DMA((COPIES,)),
        ],
        compiler_params=pltpu.CompilerParams(
            collective_id=0, has_side_effects=True, vmem_limit_bytes=60 * 1024 * 1024
        ),
    )(layer_input, output_grad, query_weight, key_weight, value_weight, out_weight, sink_logit)
    return outs[:5] + (outs[5][0, :4],)


def solution(mesh):
    placed = (
        P("sp", "tp"),
        P("sp", "tp"),
        P(None, "tp"),
        P(None, "tp"),
        P(None, "tp"),
        P("tp", None),
        P("tp"),
    )
    return jax.shard_map(
        per_device,
        mesh=mesh,
        in_specs=placed,
        out_specs=(
            P("sp", "tp"),
            P("sp", "tp"),
            P("sp", "tp"),
            P("sp", "tp"),
            P("tp", "sp"),
            P("tp"),
        ),
        check_vma=False,
    )
```

time: 364 us -> 117 us (0.32)
  the two profiles are of different devices: /device:TPU:2 before, /device:TPU:1 now
where the time goes in v1:
time: 117 us
  Pallas kernels  107 us (91%)
  local copies, waits for them, and re-layouts  9.14 us (8%)
    pallas_call x1, Pallas kernels, per_device(): pl.pallas_call(kernel, name='attention_backward', out_shape=(jax.ShapeDty...  107 us
    unnamed x5, local copies, waits for them, and re-layouts  7.95 us

profile of v1, /device:TPU:1, one launch (start us, length us, event | category | flops | bytes accessed | tf_op | source)
XLA Modules:
  0.0 117.1 jit_solution(14480326665564661341)
XLA Ops:
  0.6 107.3 %attention_backward.1 = (bf16[160,1024]{1,0:T(8,128)(2,1)}, f32[64,512]{1,0:T(8,128)}, f32[64,256]{1,0:T(8,128)}, f32[64,256]{1,0:T(8,128)}, f32[512,64]{1,0:T(8,128)}, /*index=5*/f32[8,128]{1,0:T(8,128)}) custom-call(bf16[160,1024]{1,0:T(8,128)(2,1)} %x_hbm.1, bf16[160,1024]{1,0:T(8,128)(2,1)} %g_hbm.1, bf16[4096,512]{1,0:T(8,128)(2,1)} %wq_hbm.1, ...), custom_call_target="tpu_custom_call" | custom-call | tf_op jit(solution)/shard_map/attention_backward/pallas_call | solution.py:419
  108.0 1.2 %slice_bitcast_fusion = f32[4]{0:T(128)} fusion(f32[8,128]{1,0:T(8,128)} %get-tuple-element.17), kind=kLoop, calls=%fused_computation | loop fusion | bytes 32 | tf_op jit(solution)/shard_map/squeeze | solution.py:474
  109.2 1.7 %copy.13 = f32[512,64]{0,1:T(8,128)} copy(f32[512,64]{1,0:T(8,128)} %get-tuple-element.22) | data formatting | bytes 262144
  110.9 1.7 %copy.18 = bf16[160,1024]{1,0:T(8,128)(2,1)} copy(bf16[160,1024]{1,0:T(8,128)(2,1)} %get-tuple-element.30) | data formatting | bytes 655360
  112.6 1.6 %copy.19 = f32[64,512]{1,0:T(8,128)} copy(f32[64,512]{1,0:T(8,128)} %get-tuple-element.31) | data formatting | bytes 262144
  114.2 1.5 %copy.20 = f32[64,256]{1,0:T(8,128)} copy(f32[64,256]{1,0:T(8,128)} %get-tuple-element.32) | data formatting | bytes 131072
  115.7 1.5 %copy.21 = f32[64,256]{1,0:T(8,128)} copy(f32[64,256]{1,0:T(8,128)} %get-tuple-element.33) | data formatting | bytes 131072

commit v2 on v1

v2 whole, which is shorter than its diff:
```python
import jax
import jax.numpy as jnp
from jax import lax
from jax.experimental import pallas as pl
from jax.experimental.pallas import tpu as pltpu
from jax.sharding import PartitionSpec as P

HEAD = 128
WINDOW = 128
NZ, NX, NC, NY = 8, 4, 2, 4
TOK = 160
SEQ = TOK * NZ * NX * NC
BAND = TOK + 2 * WINDOW
QC = 512
KC = 256
SCALING = HEAD ** (-0.5)
MASKED = -1e30
BF = jnp.bfloat16
F32 = jnp.float32
COPIES = 160


def mm(left, right, left_dim, right_dim):
    return lax.dot_general(
        left, right, (((left_dim,), (right_dim,)), ((), ())), preferred_element_type=F32
    )


def kernel(
    x_hbm, g_hbm, wq_hbm, wk_hbm, wv_hbm, wo_hbm, sink_ref,
    dx_out, wq_out, wk_out, wv_out, wo_out, sink_out,
    xg, dg, xc, dc, wq, wk, wv, wo, acc, dacc, band, queries, grads,
    soft, psink, gc, kvg, hs, hr, pf, pb, sr, zs, zr, ys, yr, dxo, skx, skc, skz,
    local_sem, send_sem, recv_sem,
):
    sp = lax.axis_index("sp")
    y = lax.axis_index("tp")
    z = sp // (NX * NC)
    x = lax.rem(sp // NC, NX)
    c = lax.rem(sp, NC)

    def at_y(step):
        return (sp, lax.rem(y + step, NY))

    def at_x(step):
        return ((z * NX + lax.rem(x + step, NX)) * NC + c, y)

    def at_z(step):
        return ((lax.rem(z + step, NZ) * NX + x) * NC + c, y)

    sister = (sp + 1 - 2 * c, y)
    after = (lax.rem(sp + 1, NZ * NX * NC), y)
    before = (lax.rem(sp + NZ * NX * NC - 1, NZ * NX * NC), y)
    up, down = at_y(1), at_y(3)
    right, left = at_x(1), at_x(3)

    started = []
    local_count = [0]

    def send(src, dst, device):
        k = len(started)
        copy = pltpu.make_async_remote_copy(
            src_ref=src,
            dst_ref=dst,
            send_sem=send_sem.at[k],
            recv_sem=recv_sem.at[k],
            device_id=device,
            device_id_type=pl.DeviceIdType.MESH,
        )
        copy.start()
        started.append(copy)
        return copy

    def load(src, dst):
        k = local_count[0]
        local_count[0] += 1
        copy = pltpu.make_async_copy(src, dst, local_sem.at[k])
        copy.start()
        return copy

    def loads(hbm, blocks):
        return [
            load(hbm.at[:, pl.ds(k * 128, 128)], blocks.at[0, k // 4, k % 4]) for k in range(8)
        ]

    x_loads = loads(x_hbm, xg)
    d_loads = loads(g_hbm, dg)
    weight_loads = [load(wq_hbm, wq), load(wk_hbm, wk), load(wv_hbm, wv)]
    out_load = load(wo_hbm, wo)

    barrier = pltpu.get_barrier_semaphore()
    peers = [up, down, at_y(2), right, left, at_x(2), sister, after, before, at_z(1), at_z(7)]
    for peer in peers:
        pl.semaphore_signal(
            barrier, inc=1, device_id=peer, device_id_type=pl.DeviceIdType.MESH
        )
    pl.semaphore_wait(barrier, len(peers))

    class Gather:
        def __init__(self, piece, count, plus, minus):
            self.piece, self.count, self.plus, self.minus = piece, count, plus, minus
            self.ahead, self.behind, self.far = {}, {}, []
            for i in range(count):
                k = count - 1 - i
                self.ahead[i] = send(piece(0, i), piece(1, i), plus)
                self.behind[k] = send(piece(0, k), piece(3, k), minus)

        def forward(self):
            for i in range(self.count // 2):
                k = self.count - 1 - i
                self.ahead[i].wait_recv()
                self.far.append(send(self.piece(1, i), self.piece(2, i), self.plus))
                self.behind[k].wait_recv()
                self.far.append(send(self.piece(3, k), self.piece(2, k), self.minus))

        def wait_near(self):
            for i in range(self.count // 2, self.count):
                self.ahead[i].wait_recv()
                self.behind[self.count - 1 - i].wait_recv()

        def wait_far(self):
            for copy in self.far:
                copy.wait_recv()

    def quarters(blocks):
        return lambda ry, i: blocks.at[ry, i // 2, pl.ds(2 * (i % 2), 2)]

    def exchange(blocks, cells, ry):
        copies = [
            send(blocks.at[ry, :, lax.rem(x + step, NX)], cells.at[ry, :, step], at_x(step))
            for step in (2, 1, 3)
        ]
        for h in range(2):
            cells[ry, h, 0] = blocks[ry, h, x]
        return copies

    def wide(blocks, ry):
        return jnp.concatenate([blocks[ry, h, k] for h in range(2) for k in range(4)], axis=1)

    def features(ry):
        return pl.multiple_of(lax.rem(y + NY - ry, NY) * 1024, 1024)

    def project(ry):
        rows = pl.ds(features(ry), 1024)
        block = wide(xg, ry)
        for cols, weight in (
            (slice(0, QC), wq),
            (slice(QC, QC + KC), wk),
            (slice(QC + KC, QC + 2 * KC), wv),
        ):
            term = mm(block, weight[rows, :], 1, 0)
            acc[:, cols] = term if ry == 0 else acc[:, cols] + term

    def project_grad(ry):
        cols = pl.ds(features(ry), 1024)
        term = mm(wide(dg, ry), wo[:, cols], 1, 1)
        dacc[...] = term if ry == 0 else dacc[...] + term

    for copy in x_loads:
        copy.wait()
    x_gather = Gather(quarters(xg), 4, up, down)
    x_cells = exchange(xg, xc, 0)
    for copy in d_loads:
        copy.wait()
    d_cells = exchange(dg, dc, 0)
    for copy in weight_loads:
        copy.wait()
    project(0)
    x_gather.forward()
    d_gather = Gather(quarters(dg), 4, up, down)
    x_gather.wait_near()
    x_cells += exchange(xg, xc, 1)
    x_cells += exchange(xg, xc, 3)
    project(1)
    project(3)
    x_gather.wait_far()
    x_cells += exchange(xg, xc, 2)
    project(2)

    band[WINDOW : WINDOW + TOK, :] = acc[:, QC : QC + 2 * KC].astype(BF)
    queries[...] = acc[:, :QC].astype(BF)
    halo_after = send(band.at[pl.ds(TOK, WINDOW)], band.at[pl.ds(0, WINDOW)], after)
    halo_before = send(
        band.at[pl.ds(WINDOW, WINDOW)], band.at[pl.ds(WINDOW + TOK, WINDOW)], before
    )
    d_gather.forward()
    for copy in d_cells:
        copy.wait_recv()
    dc_gather = Gather(lambda ry, h: dc.at[ry, h, pl.ds(1, 3)], 2, up, down)
    out_load.wait()
    project_grad(0)
    halo_after.wait_recv()
    halo_before.wait_recv()

    row = lax.broadcasted_iota(jnp.int32, (2 * TOK, BAND), 0)
    row = jnp.where(row >= TOK, row - TOK, row)
    col = lax.broadcasted_iota(jnp.int32, (2 * TOK, BAND), 1) - WINDOW
    key_pos = sp * TOK + col
    in_window = (jnp.abs(row - col) <= WINDOW) & (key_pos >= 0) & (key_pos < SEQ)
    second_head = lax.broadcasted_iota(jnp.int32, (2 * TOK, 1), 0) >= TOK

    def heads(ref, kh):
        cols = kh * 2 * HEAD
        return jnp.concatenate(
            [ref[:, cols : cols + HEAD], ref[:, cols + HEAD : cols + 2 * HEAD]], axis=0
        )

    def put_heads(group, kh, value):
        gc[group, 2 * kh, 0] = value[:TOK].astype(BF)
        gc[group, 2 * kh + 1, 0] = value[TOK:].astype(BF)

    for kh in range(2):
        keys = band[:, kh * HEAD : (kh + 1) * HEAD]
        values = band[:, KC + kh * HEAD : KC + (kh + 1) * HEAD]
        scores = mm(heads(queries, kh), keys, 1, 1) * SCALING
        scores = jnp.where(in_window, scores, MASKED)
        sink = jnp.where(second_head, sink_ref[2 * kh + 1], sink_ref[2 * kh])
        row_max = jnp.maximum(jnp.max(scores, axis=1, keepdims=True), sink)
        weights = jnp.exp(scores - row_max)
        sink_weight = jnp.exp(sink - row_max)
        inverse = 1.0 / (jnp.sum(weights, axis=1, keepdims=True) + sink_weight)
        weights = weights * inverse
        soft[kh] = weights
        psink[kh] = sink_weight * inverse
        put_heads(0, kh, mm(weights.astype(BF), values, 1, 0))

    def share(group):
        return Gather(lambda r, i: gc.at[group, i, r], 4, right, left)

    shares = {0: share(0)}
    d_gather.wait_near()
    for ry in (1, 3):
        project_grad(ry)
        for h in range(2):
            dc[ry, h, 0] = dg[ry, h, x]
    d_gather.wait_far()
    project_grad(2)
    for h in range(2):
        dc[2, h, 0] = dg[2, h, x]
    grads[...] = dacc[...].astype(BF)

    lane = lax.broadcasted_iota(jnp.int32, (8, 128), 1)
    sink_tile = jnp.zeros((8, 128), F32)
    for kh in range(2):
        keys = band[:, kh * HEAD : (kh + 1) * HEAD]
        values = band[:, KC + kh * HEAD : KC + (kh + 1) * HEAD]
        query = heads(queries, kh)
        grad = heads(grads, kh)
        attended = jnp.concatenate([gc[0, 2 * kh, 0], gc[0, 2 * kh + 1, 0]], axis=0)
        row_dots = jnp.sum(grad.astype(F32) * attended.astype(F32), axis=1, keepdims=True)
        weights = soft[kh]
        prob_grads = mm(grad, values, 1, 1)
        score_grads = (weights * (prob_grads - row_dots)).astype(BF)
        put_heads(1, kh, mm(score_grads, keys, 1, 0) * SCALING)
        kvg[:, kh * HEAD : (kh + 1) * HEAD] = mm(score_grads, query, 0, 0) * SCALING
        kvg[:, KC + kh * HEAD : KC + (kh + 1) * HEAD] = mm(weights.astype(BF), grad, 0, 0)
        sink_rows = psink[kh] * row_dots
        for g in range(2):
            total = -jnp.sum(sink_rows[g * TOK : (g + 1) * TOK], axis=0, keepdims=True)
            sink_tile = jnp.where(lane == 2 * kh + g, total, sink_tile)
    hs[0] = kvg[0:WINDOW, :].astype(BF)
    hs[1] = kvg[WINDOW + TOK : BAND, :].astype(BF)
    back = send(hs.at[0], hr.at[0], before)
    forth = send(hs.at[1], hr.at[1], after)
    shares[1] = share(1)
    skx[x] = sink_tile
    sink_x = [send(skx.at[x], skx.at[x], at_x(step)) for step in (1, 3, 2)]

    dc_gather.forward()
    shares[0].forward()
    back.wait_recv()
    forth.wait_recv()
    kvg[TOK : WINDOW + TOK, :] += hr[0].astype(F32)
    kvg[WINDOW : 2 * WINDOW, :] += hr[1].astype(F32)
    for k in range(4):
        gc[2, k, 0] = kvg[WINDOW : WINDOW + TOK, k * HEAD : (k + 1) * HEAD].astype(BF)
    shares[2] = share(2)

    def input_share(step):
        rows = pl.ds(pl.multiple_of(lax.rem(y + step, NY) * 1024, 1024), 1024)
        own = [jnp.concatenate([gc[g, k, 0] for k in range(4)], axis=1) for g in (1, 2)]
        return (
            mm(own[0], wq[rows, :], 1, 1)
            + mm(own[1][:, :KC], wk[rows, :], 1, 1)
            + mm(own[1][:, KC:], wv[rows, :], 1, 1)
        )

    def input_send(step):
        ys[step - 1] = input_share(step).astype(BF)
        return send(ys.at[step - 1], yr.at[step - 1], at_y(step))

    y_copies = [input_send(2)]
    shares[1].forward()
    y_copies.append(input_send(1))
    y_copies.append(input_send(3))
    dc_gather.wait_near()
    dc_gather.wait_far()
    shares[0].wait_near()
    shares[0].wait_far()

    def multiply(group, cells):
        rows = jnp.concatenate(
            [cells[ry, h].reshape(NX * TOK, 128) for ry in range(NY) for h in range(2)], axis=1
        )
        cols = jnp.concatenate(
            [gc[group, k].reshape(NX * TOK, 128) for k in range(4)], axis=1
        )
        product = mm(rows, cols, 0, 0).reshape(NY, 2, NC, 64, QC)
        pf[group] = product
        pb[group] = product.astype(BF)
        return send(pb.at[group, :, :, 1 - c], sr.at[group], sister)

    class Ring:
        def __init__(self, group, from_sister, parts):
            self.group = group
            from_sister.wait_recv()
            width = QC // parts
            self.slices = [slice(p * width, (p + 1) * width) for p in range(parts)]
            self.copies = {}
            self.hop(0)

        def own(self, step, cols):
            to = lax.rem(z + step, NZ)
            ry = lax.rem(y + NY - to // 2, NY)
            h = lax.rem(to, 2)
            mine = pf[self.group, ry, h, c, :, cols]
            return mine + sr[self.group, ry, h, :, cols].astype(F32)

        def hop(self, k):
            for p, cols in enumerate(self.slices):
                for way, step in ((0, 4 - k), (1, 5 + k)):
                    if way == 1 and k == 3:
                        continue
                    total = self.own(step, cols)
                    if k > 0:
                        self.copies[way, k - 1, p].wait_recv()
                        total = total + zr[self.group, way, k - 1, :, cols].astype(F32)
                    zs[self.group, way, k, :, cols] = total.astype(BF)
                    span = pl.ds(cols.start, cols.stop - cols.start)
                    self.copies[way, k, p] = send(
                        zs.at[self.group, way, k, :, span],
                        zr.at[self.group, way, k, :, span],
                        at_z(1 if way == 0 else 7),
                    )

        def finish(self, p):
            cols = self.slices[p]
            total = self.own(0, cols)
            for way, k in ((1, 2), (0, 3)):
                self.copies[way, k, p].wait_recv()
                total = total + zr[self.group, way, k, :, cols].astype(F32)
            return total

    s0 = multiply(0, dc)
    for copy in sink_x:
        copy.wait_recv()
    skc[c] = (skx[0] + skx[1]) + (skx[2] + skx[3])
    sink_c = send(skc.at[c], skc.at[c], sister)
    shares[2].forward()
    ring0 = Ring(0, s0, 1)
    for copy in x_cells:
        copy.wait_recv()
    shares[1].wait_near()
    shares[1].wait_far()
    s1 = multiply(1, xc)
    ring0.hop(1)
    ring1 = Ring(1, s1, 1)
    shares[2].wait_near()
    shares[2].wait_far()
    s2 = multiply(2, xc)
    sink_c.wait_recv()
    skz[z] = skc[0] + skc[1]
    sink_z = []

    def sink_hop(k):
        for way, sign in ((0, -1), (1, 1)):
            if way == 1 and k == 3:
                continue
            if k > 0:
                sink_z[2 * (k - 1) + way].wait_recv()
            tile = skz.at[lax.rem(z + NZ + sign * k, NZ)]
            sink_z.append(send(tile, tile, at_z(1 if way == 0 else 7)))

    sink_hop(0)
    ring0.hop(2)
    ring1.hop(1)
    ring2 = Ring(2, s2, 2)
    ring0.hop(3)
    sink_hop(1)
    ring1.hop(2)
    ring2.hop(1)
    dxo[...] = input_share(0)
    sink_hop(2)
    ring1.hop(3)
    ring2.hop(2)
    wo_out[...] = ring0.finish(0)
    ring2.hop(3)
    sink_hop(3)
    for copy in y_copies:
        copy.wait_recv()
    total = dxo[...]
    for k in range(3):
        total = total + yr[k].astype(F32)
    dx_out[...] = total.astype(BF)
    wq_out[...] = ring1.finish(0)
    wk_out[...] = ring2.finish(0)
    wv_out[...] = ring2.finish(1)
    for copy in sink_z[5:]:
        copy.wait_recv()
    total = skz[0]
    for k in range(1, NZ):
        total = total + skz[k]
    sink_out[...] = total
    for copy in started:
        copy.wait_send()


def finish(*refs):
    for source, target in zip(refs[:5], refs[6:11]):
        target[...] = source[...]
    refs[11][...] = refs[5][0:1, 0:4]


def per_device(
    layer_input, output_grad, query_weight, key_weight, value_weight, out_weight, sink_logit
):
    vmem = pltpu.VMEM
    outside = pl.BlockSpec(memory_space=pltpu.HBM)
    inside = pl.BlockSpec(memory_space=pltpu.VMEM)
    results = (
        jax.ShapeDtypeStruct((TOK, 1024), BF),
        jax.ShapeDtypeStruct((64, QC), F32),
        jax.ShapeDtypeStruct((64, KC), F32),
        jax.ShapeDtypeStruct((64, KC), F32),
        jax.ShapeDtypeStruct((64, QC), F32),
    )
    outs = pl.pallas_call(
        kernel,
        name="attention_backward",
        out_shape=results + (jax.ShapeDtypeStruct((8, 128), F32),),
        in_specs=[outside] * 6 + [pl.BlockSpec(memory_space=pltpu.SMEM)],
        out_specs=[inside] * 6,
        scratch_shapes=[
            vmem((NY, 2, 4, TOK, 128), BF),
            vmem((NY, 2, 4, TOK, 128), BF),
            vmem((NY, 2, NX, TOK, 128), BF),
            vmem((NY, 2, NX, TOK, 128), BF),
            vmem((4096, QC), BF),
            vmem((4096, KC), BF),
            vmem((4096, KC), BF),
            vmem((QC, 4096), BF),
            vmem((TOK, QC + 2 * KC), F32),
            vmem((TOK, QC), F32),
            vmem((BAND, 2 * KC), BF),
            vmem((TOK, QC), BF),
            vmem((TOK, QC), BF),
            vmem((2, 2 * TOK, BAND), F32),
            vmem((2, 2 * TOK, 1), F32),
            vmem((3, 4, NX, TOK, 128), BF),
            vmem((BAND, 2 * KC), F32),
            vmem((2, WINDOW, 2 * KC), BF),
            vmem((2, WINDOW, 2 * KC), BF),
            vmem((3, NY, 2, NC, 64, QC), F32),
            vmem((3, NY, 2, NC, 64, QC), BF),
            vmem((3, NY, 2, 64, QC), BF),
            vmem((3, 2, 4, 64, QC), BF),
            vmem((3, 2, 4, 64, QC), BF),
            vmem((3, TOK, 1024), BF),
            vmem((3, TOK, 1024), BF),
            vmem((TOK, 1024), F32),
            vmem((NX, 8, 128), F32),
            vmem((NC, 8, 128), F32),
            vmem((NZ, 8, 128), F32),
            pltpu.SemaphoreType.DMA((20,)),
            pltpu.SemaphoreType.DMA((COPIES,)),
            pltpu.SemaphoreType.DMA((COPIES,)),
        ],
        compiler_params=pltpu.CompilerParams(
            collective_id=0, has_side_effects=True, vmem_limit_bytes=50 * 1024 * 1024
        ),
    )(layer_input, output_grad, query_weight, key_weight, value_weight, out_weight, sink_logit)
    outs = pl.pallas_call(
        finish,
        name="finish",
        out_shape=results + (jax.ShapeDtypeStruct((1, 4), F32),),
        in_specs=[inside] * 6,
        out_specs=[inside] * 6,
        compiler_params=pltpu.CompilerParams(vmem_limit_bytes=8 * 1024 * 1024),
    )(*outs)
    return outs[:4] + (outs[4].T, outs[5].reshape(4))


def solution(mesh):
    placed = (
        P("sp", "tp"),
        P("sp", "tp"),
        P(None, "tp"),
        P(None, "tp"),
        P(None, "tp"),
        P("tp", None),
        P("tp"),
    )
    return jax.shard_map(
        per_device,
        mesh=mesh,
        in_specs=placed,
        out_specs=(
            P("sp", "tp"),
            P("sp", "tp"),
            P("sp", "tp"),
            P("sp", "tp"),
            P("tp", "sp"),
            P("tp"),
        ),
        check_vma=False,
    )
```

time: 117 us -> 81.6 us (0.70)
  the two profiles are of different devices: /device:TPU:1 before, /device:TPU:2 now
where the time goes in v2:
time: 81.6 us; the launch traced here: 81.2 us
  Pallas kernels  76.4 us (94%)
  local copies, waits for them, and re-layouts  4.18 us (5%)
    pallas_call x1, Pallas kernels, per_device(): pl.pallas_call(kernel, name='attention_backward', out_shape=results + (ja...  75.5 us
    unnamed x8, local copies, waits for them, and re-layouts  4.18 us

profile of v2, /device:TPU:2, one launch (start us, length us, event | category | flops | bytes accessed | tf_op | source)
XLA Modules:
  0.0 81.2 jit_solution(6488237581969537923)
XLA Ops:
  0.6 0.0 copy-start
  0.6 1.6 %copy-done = bf16[4096,256]{1,0:T(8,128)(2,1)S(1)} copy-done((bf16[4096,256]{1,0:T(8,128)(2,1)S(1)}, bf16[4096,256]{1,0:T(8,128)(2,1)}, u32[]{:S(2)}) %copy-start) | copy-done | bytes 2097176
  2.2 0.0 copy-start.1
  2.2 1.0 %copy-done.1 = bf16[160,1024]{1,0:T(8,128)(2,1)S(1)} copy-done((bf16[160,1024]{1,0:T(8,128)(2,1)S(1)}, bf16[160,1024]{1,0:T(8,128)(2,1)}, u32[]{:S(2)}) %copy-start.1) | copy-done | bytes 327704
  3.2 0.0 copy-start.2
  3.2 1.0 %copy-done.2 = bf16[160,1024]{1,0:T(8,128)(2,1)S(1)} copy-done((bf16[160,1024]{1,0:T(8,128)(2,1)S(1)}, bf16[160,1024]{1,0:T(8,128)(2,1)}, u32[]{:S(2)}) %copy-start.2) | copy-done | bytes 327704
  4.2 0.0 copy-start.3
  4.2 0.7 copy-done.3
  4.8 75.5 %attention_backward.1 = (bf16[160,1024]{1,0:T(8,128)(2,1)S(1)}, f32[64,512]{1,0:T(8,128)S(1)}, f32[64,256]{1,0:T(8,128)S(1)}, f32[64,256]{1,0:T(8,128)S(1)}, f32...) custom-call(bf16[160,1024]{1,0:T(8,128)(2,1)S(1)} %copy-done.1, bf16[160,1024]{1,0:T(8,128)(2,1)S(1)} %copy-done.2, ...), custom_call_target="tpu_custom_call" | custom-call | tf_op jit(solution)/shard_map/attention_backward/pallas_call | solution.py:437
  80.3 0.9 %finish.1 = (bf16[160,1024]{1,0:T(8,128)(2,1)}, f32[64,512]{1,0:T(8,128)}, f32[64,256]{1,0:T(8,128)}, f32[64,256]{1,0:T(8,128)}, f32[64,512]{1,0:T(8,128)}, /*index=5*/f32[1,4]{1,0:T(1,128)}) custom-call(bf16[160,1024]{1,0:T(8,128)(2,1)S(1)} %get-tuple-element.18.refs_0_, f32[64,512]{1,0:T(8,128)S(1)} %get-tuple-element.19.refs_1_, ...), custom_call_target="tpu_custom_call" | custom-call | tf_op jit(solution)/shard_map/finish/pallas_call | solution.py:482
Async XLA Ops:
  0.6 1.6 %copy-start = (bf16[4096,256]{1,0:T(8,128)(2,1)S(1)}, bf16[4096,256]{1,0:T(8,128)(2,1)}, u32[]{:S(2)}) copy-start(bf16[4096,256]{1,0:T(8,128)(2,1)} %wk_hbm.1) | copy-start | bytes 6291460
  2.2 1.0 %copy-start.1 = (bf16[160,1024]{1,0:T(8,128)(2,1)S(1)}, bf16[160,1024]{1,0:T(8,128)(2,1)}, u32[]{:S(2)}) copy-start(bf16[160,1024]{1,0:T(8,128)(2,1)} %x_hbm.1) | copy-start | bytes 983044
  3.2 1.0 %copy-start.2 = (bf16[160,1024]{1,0:T(8,128)(2,1)S(1)}, bf16[160,1024]{1,0:T(8,128)(2,1)}, u32[]{:S(2)}) copy-start(bf16[160,1024]{1,0:T(8,128)(2,1)} %g_hbm.1) | copy-start | bytes 983044
  4.2 0.7 copy-start.3

commit v3 on v2

--- a/solution.py
+++ b/solution.py
@@ -17,7 +17,7 @@
 MASKED = -1e30
 BF = jnp.bfloat16
 F32 = jnp.float32
-COPIES = 160
+COPIES = 176
 
 
 def mm(left, right, left_dim, right_dim):
@@ -29,8 +29,8 @@
 def kernel(
     x_hbm, g_hbm, wq_hbm, wk_hbm, wv_hbm, wo_hbm, sink_ref,
     dx_out, wq_out, wk_out, wv_out, wo_out, sink_out,
-    xg, dg, xc, dc, wq, wk, wv, wo, acc, dacc, band, queries, grads,
-    soft, psink, gc, kvg, hs, hr, pf, pb, sr, zs, zr, ys, yr, dxo, skx, skc, skz,
+    xg, dg, xc, dc, xt, dt, wq, wk, wv, wo, acc, dacc, band, queries, grads,
+    soft, psink, gc, kvg, hs, hr, pf, pb, sr, zs, zr, ys, yr, yrelay, dxo, skx, skc, skz,
     local_sem, send_sem, recv_sem,
 ):
     sp = lax.axis_index("sp")
@@ -126,8 +126,9 @@
         return lambda ry, i: blocks.at[ry, i // 2, pl.ds(2 * (i % 2), 2)]
 
     def exchange(blocks, cells, ry):
+        which = pl.ds(0, 2) if ry == 0 else 1
         copies = [
-            send(blocks.at[ry, :, lax.rem(x + step, NX)], cells.at[ry, :, step], at_x(step))
+            send(blocks.at[ry, which, lax.rem(x + step, NX)], cells.at[ry, which, step], at_x(step))
             for step in (2, 1, 3)
         ]
         for h in range(2):
@@ -174,7 +175,6 @@
     project(1)
     project(3)
     x_gather.wait_far()
-    x_cells += exchange(xg, xc, 2)
     project(2)
 
     band[WINDOW : WINDOW + TOK, :] = acc[:, QC : QC + 2 * KC].astype(BF)
@@ -183,6 +183,7 @@
     halo_before = send(
         band.at[pl.ds(WINDOW, WINDOW)], band.at[pl.ds(WINDOW + TOK, WINDOW)], before
     )
+    x_cells += exchange(xg, xc, 2)
     d_gather.forward()
     for copy in d_cells:
         copy.wait_recv()
@@ -239,6 +240,7 @@
         dc[2, h, 0] = dg[2, h, x]
     grads[...] = dacc[...].astype(BF)
 
+    shares[0].forward()
     lane = lax.broadcasted_iota(jnp.int32, (8, 128), 1)
     sink_tile = jnp.zeros((8, 128), F32)
     for kh in range(2):
@@ -262,12 +264,53 @@
     hs[1] = kvg[WINDOW + TOK : BAND, :].astype(BF)
     back = send(hs.at[0], hr.at[0], before)
     forth = send(hs.at[1], hr.at[1], after)
+    skx[x] = sink_tile
+
+    def owner(step):
+        return pl.ds(pl.multiple_of(lax.rem(y + step, NY) * 1024, 1024), 1024)
+
+    def own_grads(group):
+        return jnp.concatenate([gc[group, k, 0] for k in range(4)], axis=1)
+
+    def input_share(step):
+        own = own_grads(2)
+        return (
+            dxo[step]
+            + mm(own[:, :KC], wk[owner(step), :], 1, 1)
+            + mm(own[:, KC:], wv[owner(step), :], 1, 1)
+        )
+
+    low, high = pl.ds(0, TOK // 2), pl.ds(TOK // 2, TOK // 2)
+
+    def input_far():
+        ys[1] = input_share(2).astype(BF)
+        return [
+            send(ys.at[1, low], yrelay.at[0], up),
+            send(ys.at[1, high], yrelay.at[1], down),
+        ]
+
+    def input_near(step, block, rows, device):
+        dxo[step] = input_share(step)
+        ys[block, rows, :] = dxo[step, rows, :].astype(BF)
+        return send(ys.at[block, rows], yr.at[block // 2, rows], device)
+
+    def input_pass(copies):
+        for k, step, block, rows, device in ((0, 1, 0, low, up), (1, 3, 2, high, down)):
+            copies[k].wait_recv()
+            ys[block, rows, :] = (dxo[step, rows, :] + yrelay[k].astype(F32)).astype(BF)
+            copies.append(send(ys.at[block, rows], yr.at[block // 2, rows], device))
+
     shares[1] = share(1)
-    skx[x] = sink_tile
     sink_x = [send(skx.at[x], skx.at[x], at_x(step)) for step in (1, 3, 2)]
-
     dc_gather.forward()
-    shares[0].forward()
+    for copy in x_cells:
+        copy.wait_recv()
+    xc_gather = Gather(
+        lambda ry, i: xc.at[ry, 0, pl.ds(1, 3), pl.ds(i * (TOK // 2), TOK // 2)], 2, up, down
+    )
+    for step in (2, 1, 3, 0):
+        dxo[step] = mm(own_grads(1), wq[owner(step), :], 1, 1)
+    shares[1].forward()
     back.wait_recv()
     forth.wait_recv()
     kvg[TOK : WINDOW + TOK, :] += hr[0].astype(F32)
@@ -275,40 +318,29 @@
     for k in range(4):
         gc[2, k, 0] = kvg[WINDOW : WINDOW + TOK, k * HEAD : (k + 1) * HEAD].astype(BF)
     shares[2] = share(2)
-
-    def input_share(step):
-        rows = pl.ds(pl.multiple_of(lax.rem(y + step, NY) * 1024, 1024), 1024)
-        own = [jnp.concatenate([gc[g, k, 0] for k in range(4)], axis=1) for g in (1, 2)]
-        return (
-            mm(own[0], wq[rows, :], 1, 1)
-            + mm(own[1][:, :KC], wk[rows, :], 1, 1)
-            + mm(own[1][:, KC:], wv[rows, :], 1, 1)
-        )
-
-    def input_send(step):
-        ys[step - 1] = input_share(step).astype(BF)
-        return send(ys.at[step - 1], yr.at[step - 1], at_y(step))
-
-    y_copies = [input_send(2)]
-    shares[1].forward()
-    y_copies.append(input_send(1))
-    y_copies.append(input_send(3))
     dc_gather.wait_near()
     dc_gather.wait_far()
     shares[0].wait_near()
     shares[0].wait_far()
 
-    def multiply(group, cells):
-        rows = jnp.concatenate(
-            [cells[ry, h].reshape(NX * TOK, 128) for ry in range(NY) for h in range(2)], axis=1
-        )
-        cols = jnp.concatenate(
-            [gc[group, k].reshape(NX * TOK, 128) for k in range(4)], axis=1
-        )
-        product = mm(rows, cols, 0, 0).reshape(NY, 2, NC, 64, QC)
-        pf[group] = product
-        pb[group] = product.astype(BF)
-        return send(pb.at[group, :, :, 1 - c], sr.at[group], sister)
+    def turn(cells, turned, h):
+        for ry in range(NY):
+            turned[ry, h] = cells[ry, h].reshape(NX * TOK, 128).T
+
+    def multiply(group, turned):
+        cols = jnp.concatenate([gc[group, k].reshape(NX * TOK, 128) for k in range(4)], axis=1)
+
+        def product(core):
+            rows = pl.ds(pl.multiple_of(core * 64, 64), 64)
+            left = jnp.concatenate(
+                [turned[ry, h, rows, :] for ry in range(NY) for h in range(2)], axis=0
+            )
+            return mm(left, cols, 1, 0).reshape(NY, 2, 64, QC)
+
+        pb[group] = product(1 - c).astype(BF)
+        copy = send(pb.at[group], sr.at[group], sister)
+        pf[group] = product(c)
+        return copy
 
     class Ring:
         def __init__(self, group, from_sister, parts):
@@ -323,7 +355,7 @@
             to = lax.rem(z + step, NZ)
             ry = lax.rem(y + NY - to // 2, NY)
             h = lax.rem(to, 2)
-            mine = pf[self.group, ry, h, c, :, cols]
+            mine = pf[self.group, ry, h, :, cols]
             return mine + sr[self.group, ry, h, :, cols].astype(F32)
 
         def hop(self, k):
@@ -331,6 +363,9 @@
                 for way, step in ((0, 4 - k), (1, 5 + k)):
                     if way == 1 and k == 3:
                         continue
+                    toward = 1 if way == 0 else 7
+                    if p % 2 == 1:
+                        step, toward = NZ - step, NZ - toward
                     total = self.own(step, cols)
                     if k > 0:
                         self.copies[way, k - 1, p].wait_recv()
@@ -340,7 +375,7 @@
                     self.copies[way, k, p] = send(
                         zs.at[self.group, way, k, :, span],
                         zr.at[self.group, way, k, :, span],
-                        at_z(1 if way == 0 else 7),
+                        at_z(toward),
                     )
 
         def finish(self, p):
@@ -351,23 +386,30 @@
                 total = total + zr[self.group, way, k, :, cols].astype(F32)
             return total
 
-    s0 = multiply(0, dc)
+    xc_gather.forward()
+    turn(dc, dt, 0)
+    turn(dc, dt, 1)
+    s0 = multiply(0, dt)
     for copy in sink_x:
         copy.wait_recv()
     skc[c] = (skx[0] + skx[1]) + (skx[2] + skx[3])
     sink_c = send(skc.at[c], skc.at[c], sister)
-    shares[2].forward()
-    ring0 = Ring(0, s0, 1)
-    for copy in x_cells:
-        copy.wait_recv()
+    turn(xc, xt, 1)
+    ring0 = Ring(0, s0, 2)
+    xc_gather.wait_near()
+    xc_gather.wait_far()
+    turn(xc, xt, 0)
     shares[1].wait_near()
     shares[1].wait_far()
-    s1 = multiply(1, xc)
+    shares[2].forward()
+    s1 = multiply(1, xt)
+    y_copies = input_far()
     ring0.hop(1)
-    ring1 = Ring(1, s1, 1)
+    ring1 = Ring(1, s1, 2)
+    y_copies.append(input_near(1, 0, high, up))
     shares[2].wait_near()
     shares[2].wait_far()
-    s2 = multiply(2, xc)
+    s2 = multiply(2, xt)
     sink_c.wait_recv()
     skz[z] = skc[0] + skc[1]
     sink_z = []
@@ -384,33 +426,38 @@
     sink_hop(0)
     ring0.hop(2)
     ring1.hop(1)
-    ring2 = Ring(2, s2, 2)
+    ring2 = Ring(2, s2, 4)
+    y_copies.append(input_near(3, 2, low, down))
+    sink_hop(1)
     ring0.hop(3)
-    sink_hop(1)
     ring1.hop(2)
     ring2.hop(1)
-    dxo[...] = input_share(0)
+    input_pass(y_copies)
+    dxo[0] = input_share(0)
     sink_hop(2)
     ring1.hop(3)
     ring2.hop(2)
-    wo_out[...] = ring0.finish(0)
+    sink_hop(3)
+    for p, cols in enumerate(ring0.slices):
+        wo_out[:, cols] = ring0.finish(p)
     ring2.hop(3)
-    sink_hop(3)
-    for copy in y_copies:
+    for copy in y_copies[2:]:
         copy.wait_recv()
-    total = dxo[...]
-    for k in range(3):
+    total = dxo[0]
+    for k in range(2):
         total = total + yr[k].astype(F32)
     dx_out[...] = total.astype(BF)
-    wq_out[...] = ring1.finish(0)
-    wk_out[...] = ring2.finish(0)
-    wv_out[...] = ring2.finish(1)
+    for p, cols in enumerate(ring1.slices):
+        wq_out[:, cols] = ring1.finish(p)
     for copy in sink_z[5:]:
         copy.wait_recv()
     total = skz[0]
     for k in range(1, NZ):
         total = total + skz[k]
     sink_out[...] = total
+    for p in range(2):
+        wk_out[:, ring2.slices[p]] = ring2.finish(p)
+        wv_out[:, ring2.slices[p]] = ring2.finish(p + 2)
     for copy in started:
         copy.wait_send()
 
@@ -445,6 +492,8 @@
             vmem((NY, 2, 4, TOK, 128), BF),
             vmem((NY, 2, NX, TOK, 128), BF),
             vmem((NY, 2, NX, TOK, 128), BF),
+        vmem((NY, 2, 128, NX * TOK), BF),
+        vmem((NY, 2, 128, NX * TOK), BF),
             vmem((4096, QC), BF),
             vmem((4096, KC), BF),
             vmem((4096, KC), BF),
@@ -460,14 +509,15 @@
             vmem((BAND, 2 * KC), F32),
             vmem((2, WINDOW, 2 * KC), BF),
             vmem((2, WINDOW, 2 * KC), BF),
-            vmem((3, NY, 2, NC, 64, QC), F32),
-            vmem((3, NY, 2, NC, 64, QC), BF),
+            vmem((3, NY, 2, 64, QC), F32),
+            vmem((3, NY, 2, 64, QC), BF),
             vmem((3, NY, 2, 64, QC), BF),
             vmem((3, 2, 4, 64, QC), BF),
             vmem((3, 2, 4, 64, QC), BF),
             vmem((3, TOK, 1024), BF),
-            vmem((3, TOK, 1024), BF),
-            vmem((TOK, 1024), F32),
+            vmem((2, TOK, 1024), BF),
+        vmem((2, TOK // 2, 1024), BF),
+            vmem((NY, TOK, 1024), F32),
             vmem((NX, 8, 128), F32),
             vmem((NC, 8, 128), F32),
             vmem((NZ, 8, 128), F32),
@@ -476,7 +526,7 @@
             pltpu.SemaphoreType.DMA((COPIES,)),
         ],
         compiler_params=pltpu.CompilerParams(
-            collective_id=0, has_side_effects=True, vmem_limit_bytes=50 * 1024 * 1024
+            collective_id=0, has_side_effects=True, vmem_limit_bytes=53 * 1024 * 1024
         ),
     )(layer_input, output_grad, query_weight, key_weight, value_weight, out_weight, sink_logit)
     outs = pl.pallas_call(

time: 81.6 us -> 73.9 us (0.906)
  Pallas kernels: 76.4 us -> 72.5 us
  local copies, waits for them, and re-layouts: 4.18 us -> 0.65 us
    pallas_call x1, Pallas kernels: 75.5 us -> 71.6 us  [per_device(): pl.pallas_call(kernel, name='attention_backward', out_shape=results + (ja...]
    unnamed x8 -> x2, local copies, waits for them, and re-layouts: 4.18 us -> 0.65 us
where the time goes in v3:
time: 73.9 us; the launch traced here: 73.8 us
  Pallas kernels  72.5 us (98%)
    pallas_call x1, Pallas kernels, per_device(): pl.pallas_call(kernel, name='attention_backward', out_shape=results + (ja...  71.6 us

profile of v3, /device:TPU:2, one launch (start us, length us, event | category | flops | bytes accessed | tf_op | source)
XLA Modules:
  0.0 73.8 jit_solution(2156634192203383691)
XLA Ops:
  0.6 0.0 copy-start
  0.6 0.6 copy-done
  1.3 71.6 %attention_backward.1 = (bf16[160,1024]{1,0:T(8,128)(2,1)S(1)}, f32[64,512]{1,0:T(8,128)S(1)}, f32[64,256]{1,0:T(8,128)S(1)}, f32[64,256]{1,0:T(8,128)S(1)}, f32...) custom-call(bf16[160,1024]{1,0:T(8,128)(2,1)} %x_hbm.1, bf16[160,1024]{1,0:T(8,128)(2,1)} %g_hbm.1, bf16[4096,512]{1,0:T(8,128)(2,1)} %wq_hbm.1, ...), custom_call_target="tpu_custom_call" | custom-call | tf_op jit(solution)/shard_map/attention_backward/pallas_call | solution.py:484
  72.9 0.9 %finish.1 = (bf16[160,1024]{1,0:T(8,128)(2,1)}, f32[64,512]{1,0:T(8,128)}, f32[64,256]{1,0:T(8,128)}, f32[64,256]{1,0:T(8,128)}, f32[64,512]{1,0:T(8,128)}, /*index=5*/f32[1,4]{1,0:T(1,128)}) custom-call(bf16[160,1024]{1,0:T(8,128)(2,1)S(1)} %get-tuple-element.18.refs_0_, f32[64,512]{1,0:T(8,128)S(1)} %get-tuple-element.19.refs_1_, ...), custom_call_target="tpu_custom_call" | custom-call | tf_op jit(solution)/shard_map/finish/pallas_call | solution.py:532
Async XLA Ops:
  0.6 0.7 copy-start

commit v4 on v3

--- a/solution.py
+++ b/solution.py
@@ -89,7 +89,7 @@
     out_load = load(wo_hbm, wo)
 
     barrier = pltpu.get_barrier_semaphore()
-    peers = [up, down, at_y(2), right, left, at_x(2), sister, after, before, at_z(1), at_z(7)]
+    peers = [up, down, right, left, at_x(2), sister, after, before, at_z(1), at_z(7)]
     for peer in peers:
         pl.semaphore_signal(
             barrier, inc=1, device_id=peer, device_id_type=pl.DeviceIdType.MESH
@@ -308,8 +308,14 @@
     xc_gather = Gather(
         lambda ry, i: xc.at[ry, 0, pl.ds(1, 3), pl.ds(i * (TOK // 2), TOK // 2)], 2, up, down
     )
+    def turn(cells, turned, blocks):
+        for ry, h in blocks:
+            turned[ry, h] = cells[ry, h].reshape(NX * TOK, 128).T
+
     for step in (2, 1, 3, 0):
         dxo[step] = mm(own_grads(1), wq[owner(step), :], 1, 1)
+    turn(xc, xt, ((0, 0), (0, 1), (1, 1), (2, 1), (3, 1)))
+    turn(dc, dt, ((0, 0), (0, 1), (1, 0), (3, 1)))
     shares[1].forward()
     back.wait_recv()
     forth.wait_recv()
@@ -322,10 +328,6 @@
     dc_gather.wait_far()
     shares[0].wait_near()
     shares[0].wait_far()
-
-    def turn(cells, turned, h):
-        for ry in range(NY):
-            turned[ry, h] = cells[ry, h].reshape(NX * TOK, 128).T
 
     def multiply(group, turned):
         cols = jnp.concatenate([gc[group, k].reshape(NX * TOK, 128) for k in range(4)], axis=1)
@@ -387,25 +389,23 @@
             return total
 
     xc_gather.forward()
-    turn(dc, dt, 0)
-    turn(dc, dt, 1)
+    turn(dc, dt, ((1, 1), (3, 0), (2, 0), (2, 1)))
     s0 = multiply(0, dt)
     for copy in sink_x:
         copy.wait_recv()
     skc[c] = (skx[0] + skx[1]) + (skx[2] + skx[3])
     sink_c = send(skc.at[c], skc.at[c], sister)
-    turn(xc, xt, 1)
     ring0 = Ring(0, s0, 2)
     xc_gather.wait_near()
     xc_gather.wait_far()
-    turn(xc, xt, 0)
+    turn(xc, xt, ((1, 0), (2, 0), (3, 0)))
     shares[1].wait_near()
     shares[1].wait_far()
     shares[2].forward()
     s1 = multiply(1, xt)
-    y_copies = input_far()
     ring0.hop(1)
     ring1 = Ring(1, s1, 2)
+    y_copies = input_far()
     y_copies.append(input_near(1, 0, high, up))
     shares[2].wait_near()
     shares[2].wait_far()
@@ -425,18 +425,18 @@
 
     sink_hop(0)
     ring0.hop(2)
+    ring2 = Ring(2, s2, 4)
     ring1.hop(1)
-    ring2 = Ring(2, s2, 4)
     y_copies.append(input_near(3, 2, low, down))
     sink_hop(1)
     ring0.hop(3)
+    ring2.hop(1)
     ring1.hop(2)
-    ring2.hop(1)
     input_pass(y_copies)
     dxo[0] = input_share(0)
     sink_hop(2)
+    ring2.hop(2)
     ring1.hop(3)
-    ring2.hop(2)
     sink_hop(3)
     for p, cols in enumerate(ring0.slices):
         wo_out[:, cols] = ring0.finish(p)

time: 73.9 us -> 72.2 us (0.977)
  Pallas kernels: 72.5 us -> 70.8 us
    pallas_call x1, Pallas kernels: 71.6 us -> 69.9 us  [per_device(): pl.pallas_call(kernel, name='attention_backward', out_shape=results + (ja...]
where the time goes in v4:
time: 72.2 us; the launch traced here: 72.1 us
  Pallas kernels  70.8 us (98%)
    pallas_call x1, Pallas kernels, per_device(): pl.pallas_call(kernel, name='attention_backward', out_shape=results + (ja...  69.9 us

profile of v4, /device:TPU:2, one launch (start us, length us, event | category | flops | bytes accessed | tf_op | source)
XLA Modules:
  0.0 72.1 jit_solution(16154921613311162549)
XLA Ops:
  0.6 0.0 copy-start
  0.6 0.6 copy-done
  1.3 69.9 %attention_backward.1 = (bf16[160,1024]{1,0:T(8,128)(2,1)S(1)}, f32[64,512]{1,0:T(8,128)S(1)}, f32[64,256]{1,0:T(8,128)S(1)}, f32[64,256]{1,0:T(8,128)S(1)}, f32...) custom-call(bf16[160,1024]{1,0:T(8,128)(2,1)} %x_hbm.1, bf16[160,1024]{1,0:T(8,128)(2,1)} %g_hbm.1, bf16[4096,512]{1,0:T(8,128)(2,1)} %wq_hbm.1, ...), custom_call_target="tpu_custom_call" | custom-call | tf_op jit(solution)/shard_map/attention_backward/pallas_call | solution.py:484
  71.2 0.9 %finish.1 = (bf16[160,1024]{1,0:T(8,128)(2,1)}, f32[64,512]{1,0:T(8,128)}, f32[64,256]{1,0:T(8,128)}, f32[64,256]{1,0:T(8,128)}, f32[64,512]{1,0:T(8,128)}, /*index=5*/f32[1,4]{1,0:T(1,128)}) custom-call(bf16[160,1024]{1,0:T(8,128)(2,1)S(1)} %get-tuple-element.18.refs_0_, f32[64,512]{1,0:T(8,128)S(1)} %get-tuple-element.19.refs_1_, ...), custom_call_target="tpu_custom_call" | custom-call | tf_op jit(solution)/shard_map/finish/pallas_call | solution.py:532
Async XLA Ops:
  0.6 0.7 copy-start

commit v5 on v4

--- a/solution.py
+++ b/solution.py
@@ -126,10 +126,9 @@
         return lambda ry, i: blocks.at[ry, i // 2, pl.ds(2 * (i % 2), 2)]
 
     def exchange(blocks, cells, ry):
-        which = pl.ds(0, 2) if ry == 0 else 1
         copies = [
-            send(blocks.at[ry, which, lax.rem(x + step, NX)], cells.at[ry, which, step], at_x(step))
-            for step in (2, 1, 3)
+            send(blocks.at[ry, :, lax.rem(x + step, NX)], cells.at[ry, :, step], at_x(step))
+            for step in ((2, 1, 3) if ry == 0 else (1, 3))
         ]
         for h in range(2):
             cells[ry, h, 0] = blocks[ry, h, x]
@@ -305,16 +304,14 @@
     dc_gather.forward()
     for copy in x_cells:
         copy.wait_recv()
-    xc_gather = Gather(
-        lambda ry, i: xc.at[ry, 0, pl.ds(1, 3), pl.ds(i * (TOK // 2), TOK // 2)], 2, up, down
-    )
+    xc_gather = Gather(lambda ry, h: xc.at[ry, h, 2], 2, up, down)
     def turn(cells, turned, blocks):
         for ry, h in blocks:
             turned[ry, h] = cells[ry, h].reshape(NX * TOK, 128).T
 
     for step in (2, 1, 3, 0):
         dxo[step] = mm(own_grads(1), wq[owner(step), :], 1, 1)
-    turn(xc, xt, ((0, 0), (0, 1), (1, 1), (2, 1), (3, 1)))
+    turn(xc, xt, ((0, 0), (0, 1)))
     turn(dc, dt, ((0, 0), (0, 1), (1, 0), (3, 1)))
     shares[1].forward()
     back.wait_recv()
@@ -398,7 +395,7 @@
     ring0 = Ring(0, s0, 2)
     xc_gather.wait_near()
     xc_gather.wait_far()
-    turn(xc, xt, ((1, 0), (2, 0), (3, 0)))
+    turn(xc, xt, [(ry, h) for ry in (1, 2, 3) for h in range(2)])
     shares[1].wait_near()
     shares[1].wait_far()
     shares[2].forward()

time: 72.2 us -> 72.2 us (level)
  no operation moved by 1% of the time
where the time goes in v5:
time: 72.2 us; the launch traced here: 72.1 us
  Pallas kernels  70.8 us (98%)
    pallas_call x1, Pallas kernels, per_device(): pl.pallas_call(kernel, name='attention_backward', out_shape=results + (ja...  69.9 us

profile of v5, /device:TPU:2, one launch (start us, length us, event | category | flops | bytes accessed | tf_op | source)
XLA Modules:
  0.0 72.1 jit_solution(1285187729923529378)
XLA Ops:
  0.6 0.0 copy-start
  0.6 0.6 copy-done
  1.3 69.9 %attention_backward.1 = (bf16[160,1024]{1,0:T(8,128)(2,1)S(1)}, f32[64,512]{1,0:T(8,128)S(1)}, f32[64,256]{1,0:T(8,128)S(1)}, f32[64,256]{1,0:T(8,128)S(1)}, f32...) custom-call(bf16[160,1024]{1,0:T(8,128)(2,1)} %x_hbm.1, bf16[160,1024]{1,0:T(8,128)(2,1)} %g_hbm.1, bf16[4096,512]{1,0:T(8,128)(2,1)} %wq_hbm.1, ...), custom_call_target="tpu_custom_call" | custom-call | tf_op jit(solution)/shard_map/attention_backward/pallas_call | solution.py:481
  71.2 0.9 %finish.1 = (bf16[160,1024]{1,0:T(8,128)(2,1)}, f32[64,512]{1,0:T(8,128)}, f32[64,256]{1,0:T(8,128)}, f32[64,256]{1,0:T(8,128)}, f32[64,512]{1,0:T(8,128)}, /*index=5*/f32[1,4]{1,0:T(1,128)}) custom-call(bf16[160,1024]{1,0:T(8,128)(2,1)S(1)} %get-tuple-element.18.refs_0_, f32[64,512]{1,0:T(8,128)S(1)} %get-tuple-element.19.refs_1_, ...), custom_call_target="tpu_custom_call" | custom-call | tf_op jit(solution)/shard_map/finish/pallas_call | solution.py:529
Async XLA Ops:
  0.6 0.7 copy-start

commit v6 on v5

--- a/solution.py
+++ b/solution.py
@@ -30,7 +30,7 @@
     x_hbm, g_hbm, wq_hbm, wk_hbm, wv_hbm, wo_hbm, sink_ref,
     dx_out, wq_out, wk_out, wv_out, wo_out, sink_out,
     xg, dg, xc, dc, xt, dt, wq, wk, wv, wo, acc, dacc, band, queries, grads,
-    soft, psink, gc, kvg, hs, hr, pf, pb, sr, zs, zr, ys, yr, yrelay, dxo, skx, skc, skz,
+    soft, psink, bias, gc, kvg, hs, hr, pf, pb, sr, zs, zr, ys, yr, yrelay, dxo, skx, skc, skz,
     local_sem, send_sem, recv_sem,
 ):
     sp = lax.axis_index("sp")
@@ -189,14 +189,12 @@
     dc_gather = Gather(lambda ry, h: dc.at[ry, h, pl.ds(1, 3)], 2, up, down)
     out_load.wait()
     project_grad(0)
-    halo_after.wait_recv()
-    halo_before.wait_recv()
-
     row = lax.broadcasted_iota(jnp.int32, (2 * TOK, BAND), 0)
     row = jnp.where(row >= TOK, row - TOK, row)
     col = lax.broadcasted_iota(jnp.int32, (2 * TOK, BAND), 1) - WINDOW
     key_pos = sp * TOK + col
     in_window = (jnp.abs(row - col) <= WINDOW) & (key_pos >= 0) & (key_pos < SEQ)
+    bias[...] = jnp.where(in_window, 0.0, MASKED)
     second_head = lax.broadcasted_iota(jnp.int32, (2 * TOK, 1), 0) >= TOK
 
     def heads(ref, kh):
@@ -209,11 +207,14 @@
         gc[group, 2 * kh, 0] = value[:TOK].astype(BF)
         gc[group, 2 * kh + 1, 0] = value[TOK:].astype(BF)
 
+    halo_after.wait_recv()
+    halo_before.wait_recv()
+
     for kh in range(2):
         keys = band[:, kh * HEAD : (kh + 1) * HEAD]
         values = band[:, KC + kh * HEAD : KC + (kh + 1) * HEAD]
         scores = mm(heads(queries, kh), keys, 1, 1) * SCALING
-        scores = jnp.where(in_window, scores, MASKED)
+        scores = jnp.where(bias[...] < 0.0, MASKED, scores)
         sink = jnp.where(second_head, sink_ref[2 * kh + 1], sink_ref[2 * kh])
         row_max = jnp.maximum(jnp.max(scores, axis=1, keepdims=True), sink)
         weights = jnp.exp(scores - row_max)
@@ -326,7 +327,7 @@
     shares[0].wait_near()
     shares[0].wait_far()
 
-    def multiply(group, turned):
+    def multiply(group, turned, between=None):
         cols = jnp.concatenate([gc[group, k].reshape(NX * TOK, 128) for k in range(4)], axis=1)
 
         def product(core):
@@ -338,6 +339,8 @@
 
         pb[group] = product(1 - c).astype(BF)
         copy = send(pb.at[group], sr.at[group], sister)
+        if between is not None:
+            between()
         pf[group] = product(c)
         return copy
 
@@ -385,9 +388,8 @@
                 total = total + zr[self.group, way, k, :, cols].astype(F32)
             return total
 
-    xc_gather.forward()
     turn(dc, dt, ((1, 1), (3, 0), (2, 0), (2, 1)))
-    s0 = multiply(0, dt)
+    s0 = multiply(0, dt, xc_gather.forward)
     for copy in sink_x:
         copy.wait_recv()
     skc[c] = (skx[0] + skx[1]) + (skx[2] + skx[3])
@@ -502,6 +504,7 @@
             vmem((TOK, QC), BF),
             vmem((2, 2 * TOK, BAND), F32),
             vmem((2, 2 * TOK, 1), F32),
+        vmem((2 * TOK, BAND), F32),
             vmem((3, 4, NX, TOK, 128), BF),
             vmem((BAND, 2 * KC), F32),
             vmem((2, WINDOW, 2 * KC), BF),

time: 72.2 us -> 72.4 us (level)
  no operation moved by 1% of the time
where the time goes in v6:
time: 72.4 us; the launch traced here: 72.3 us
  Pallas kernels  71 us (98%)
    pallas_call x1, Pallas kernels, per_device(): pl.pallas_call(kernel, name='attention_backward', out_shape=results + (ja...  70.1 us

profile of v6, /device:TPU:2, one launch (start us, length us, event | category | flops | bytes accessed | tf_op | source)
XLA Modules:
  0.0 72.3 jit_solution(10766437319196878413)
XLA Ops:
  0.6 0.0 copy-start
  0.6 0.6 copy-done
  1.3 70.1 %attention_backward.1 = (bf16[160,1024]{1,0:T(8,128)(2,1)S(1)}, f32[64,512]{1,0:T(8,128)S(1)}, f32[64,256]{1,0:T(8,128)S(1)}, f32[64,256]{1,0:T(8,128)S(1)}, f32...) custom-call(bf16[160,1024]{1,0:T(8,128)(2,1)} %x_hbm.1, bf16[160,1024]{1,0:T(8,128)(2,1)} %g_hbm.1, bf16[4096,512]{1,0:T(8,128)(2,1)} %wq_hbm.1, ...), custom_call_target="tpu_custom_call" | custom-call | tf_op jit(solution)/shard_map/attention_backward/pallas_call | solution.py:483
  71.4 0.9 %finish.1 = (bf16[160,1024]{1,0:T(8,128)(2,1)}, f32[64,512]{1,0:T(8,128)}, f32[64,256]{1,0:T(8,128)}, f32[64,256]{1,0:T(8,128)}, f32[64,512]{1,0:T(8,128)}, /*index=5*/f32[1,4]{1,0:T(1,128)}) custom-call(bf16[160,1024]{1,0:T(8,128)(2,1)S(1)} %get-tuple-element.18.refs_0_, f32[64,512]{1,0:T(8,128)S(1)} %get-tuple-element.19.refs_1_, ...), custom_call_target="tpu_custom_call" | custom-call | tf_op jit(solution)/shard_map/finish/pallas_call | solution.py:532
Async XLA Ops:
  0.6 0.7 copy-start
